TPU v7x, 256 devices: a whole 4x4x8 slice. The times are simulated.
256 devices in a mesh: ep: 128 (over z, y, x), tp: 2 (over core).
Axes of the slice: x: 4, y: 4, z: 8, core: 2. Of those that a mesh axis runs over, the one named last changes fastest.
Arguments:
- tokens: bfloat16 [16384, 2048], P('ep', 'tp'), may hold values from -24 to 24
- cotangent: bfloat16 [16384, 2048], P('ep', 'tp'), may hold values from -24 to 24
- routes: int32 [16384, 2], P('ep'), may hold values from 0 to 127, all different within a row; in each aligned block of 128 rows (0 to 127, 128 to 255, ...) at most 3 rows name the same one
- route_weights: float32 [16384, 2], P('ep'), may hold values from 0.1 to 2.5
- gate_proj: bfloat16 [128, 2048, 512], P('ep', None, 'tp'), may hold values from -0.125 to 0.125
- up_proj: bfloat16 [128, 2048, 512], P('ep', None, 'tp'), may hold values from -0.125 to 0.125
- down_proj: bfloat16 [128, 512, 2048], P('ep', 'tp'), may hold values from -0.25 to 0.25
- shared_gate: bfloat16 [2048, 512], P(None, 'tp'), may hold values from -0.125 to 0.125
- shared_up: bfloat16 [2048, 512], P(None, 'tp'), may hold values from -0.125 to 0.125
- shared_down: bfloat16 [2048, 512], P(None, 'tp'), may hold values from -0.25 to 0.25
Outputs:
- token_grad: bfloat16 [16384, 2048], P('ep', 'tp')
- weight_grad: float32 [16384, 2], P('ep')
- gate_grad: bfloat16 [128, 2048, 512], P('ep', None, 'tp')
- up_grad: bfloat16 [128, 2048, 512], P('ep', None, 'tp')
- down_grad: bfloat16 [128, 512, 2048], P('ep', 'tp')
- sharedgate_grad: float32 [2048, 512], P('ep', 'tp')
- sharedup_grad: float32 [2048, 512], P('ep', 'tp')
- shareddown_grad: float32 [2048, 512], P('ep', 'tp')
Inputs may be any that keep to these rules, and one draw needn't show every extreme that they name: `routes`: the 2 entries of a token name different experts. Among the 128 tokens of one group no expert is named more than 3 times, and in some groups an expert is named exactly 3 times.
All inputs are finite; a program needn't handle non-finite values.
Results may differ from a plain program's by a relative error of at most 0.007.
Values may be sent and summed in bfloat16 or wider, within the bound.
A program may use at most 128 MiB of HBM per device.

v0:
```python
import math

import jax
import jax.numpy as jnp
from jax import lax
from jax.sharding import Mesh
from jax.sharding import PartitionSpec as P

EP = ("ep_0", "ep_1", "ep_2")


def sent_together(arrays, axis, dim, along):
    widths = [a.shape[along] for a in arrays]
    both = jnp.concatenate(arrays, axis=along)
    filled = lax.all_gather(both, axis, axis=dim, tiled=True)
    return tuple(jnp.split(filled, [sum(widths[:k]) for k in range(1, len(widths))], axis=along))


def side_by_side(arrays, axis, split_dim, concat_dim, along):
    widths = [a.shape[along] for a in arrays]
    both = jnp.concatenate(arrays, axis=along)
    filled = lax.all_to_all(both, axis, split_axis=split_dim, concat_axis=concat_dim, tiled=True)
    return tuple(jnp.split(filled, [sum(widths[:k]) for k in range(1, len(widths))], axis=along))


def split_up(shard, dim, peers):
    lengths = shard.shape
    blocks = shard.reshape(*lengths[:dim], peers, lengths[dim] // peers, *lengths[dim + 1 :])
    return jnp.moveaxis(blocks, dim, 0)


def sum_at_owner(shard, axis, dim):
    peers = lax.axis_size(axis)
    blocks = lax.all_to_all(split_up(shard, dim, peers), axis, 0, 0, tiled=True)
    return jnp.sum(blocks.astype(jnp.float32), axis=0)


def side_by_side_2(arrays, axis, dim, along):
    both = jnp.concatenate(arrays, axis=along)
    filled, at, outs = (sum_at_owner(both, axis, dim), 0, [])
    for a in arrays:
        outs.append(lax.slice_in_dim(filled, at, at + a.shape[along], axis=along))
        at += a.shape[along]
    return tuple(outs)


def in_one_piece(arrays, axis, split_dim, concat_dim, along):
    widths = [math.prod(a.shape[along:]) for a in arrays]
    both = jnp.concatenate(
        [a.reshape(*a.shape[:along], w) for a, w in zip(arrays, widths)], axis=along
    )
    filled = lax.all_to_all(both, axis, split_axis=split_dim, concat_axis=concat_dim, tiled=True)
    blocks = jnp.split(filled, [sum(widths[:k]) for k in range(1, len(widths))], axis=along)
    return tuple(
        (b.reshape(*filled.shape[:along], *a.shape[along:]) for a, b in zip(arrays, blocks))
    )


def own_rows(running, axes):
    for axis in axes:
        running = lax.psum_scatter(running, axis, scatter_dimension=0, tiled=True)
    return running


def slot_table(routes, experts, capacity):
    assigned = routes.shape[0] * routes.shape[1]
    flat_routes = routes.reshape(assigned)
    onehot = (flat_routes[:, None] == jnp.arange(experts, dtype=jnp.int32)[None, :]).astype(
        jnp.int32
    )
    before = jnp.cumsum(onehot, axis=0) - onehot
    slot_rank = jnp.sum(before * onehot, axis=1)
    slot_of = flat_routes * capacity + slot_rank
    empty = jnp.full((experts * capacity,), assigned, jnp.int32)
    slot_owner = empty.at[slot_of].set(jnp.arange(assigned, dtype=jnp.int32))
    return (slot_of, slot_owner)


def silu_parts(preact):
    sigmoid_v = jax.nn.sigmoid(preact)
    return (preact * sigmoid_v, sigmoid_v * (1.0 + preact * (1.0 - sigmoid_v)))


def rounded(partial_value):
    return lax.optimization_barrier(partial_value.astype(jnp.bfloat16)).astype(jnp.float32)


def contract_rows(left, right):
    return lax.dot_general(
        left, right, (((0,), (0,)), ((), ())), preferred_element_type=jnp.float32
    )


def contract_cols(left, right):
    return lax.dot_general(
        left, right, (((1,), (1,)), ((), ())), preferred_element_type=jnp.float32
    )


def per_device(
    tokens,
    cotangent,
    routes,
    route_weights,
    gate_proj,
    up_proj,
    down_proj,
    shared_gate,
    shared_up,
    shared_down,
):
    groups = lax.axis_size(EP)
    halves = lax.axis_size("tp")
    local_count = gate_proj.shape[0]
    experts = groups * local_count
    token_rows, top = routes.shape
    assigned = token_rows * top
    capacity = assigned // experts + assigned // (2 * experts)
    per_peer = local_count * capacity
    whole_rows, whole_cot = sent_together((tokens, cotangent), "tp", 1, 0)
    slot_of, slot_owner = slot_table(routes, experts, capacity)
    filled = slot_owner < assigned
    owner_safe = jnp.minimum(slot_owner, assigned - 1)
    slot_token = owner_safe // top
    slot_weight = jnp.where(
        filled, route_weights.reshape(assigned)[owner_safe], jnp.zeros((), jnp.float32)
    )
    col_count = tokens.shape[1]
    packed_rows = jnp.where(filled[:, None], tokens[slot_token], jnp.zeros((), jnp.bfloat16))
    packed_cot = (slot_weight[:, None] * cotangent[slot_token].astype(jnp.float32)).astype(
        jnp.bfloat16
    )
    sent_rows = packed_rows.reshape(groups, per_peer, col_count)
    sent_cot = packed_cot.reshape(groups, per_peer, col_count)
    half_rows, half_cot = side_by_side((sent_rows, sent_cot), EP, 0, 0, 1)
    got_rows, got_cot = sent_together((half_rows, half_cot), "tp", 2, 0)

    def by_expert(layout):
        return jnp.swapaxes(layout.reshape(groups, local_count, capacity, -1), 0, 1).reshape(
            local_count, groups * capacity, -1
        )

    def by_peer(layout):
        return jnp.swapaxes(layout.reshape(local_count, groups, capacity, -1), 0, 1).reshape(
            groups * per_peer, -1
        )

    slot_rows = by_expert(got_rows)
    slot_cot = by_expert(got_cot)
    gate_pre = jnp.einsum("erd,edf->erf", slot_rows, gate_proj, preferred_element_type=jnp.float32)
    up_pre = jnp.einsum("erd,edf->erf", slot_rows, up_proj, preferred_element_type=jnp.float32)
    gate_act, gate_slope = silu_parts(gate_pre)
    hidden = gate_act * up_pre
    back_grad = jnp.einsum("erd,efd->erf", slot_cot, down_proj, preferred_element_type=jnp.float32)
    product = jnp.sum(hidden * back_grad, axis=2, keepdims=True)
    hidden_low = hidden.astype(jnp.bfloat16)
    down_grad = jnp.einsum(
        "erf,erd->efd", hidden_low, slot_cot, preferred_element_type=jnp.float32
    ).astype(jnp.bfloat16)
    gate_delta = (back_grad * up_pre * gate_slope).astype(jnp.bfloat16)
    up_delta = (back_grad * gate_act).astype(jnp.bfloat16)
    gate_grad = jnp.einsum(
        "erd,erf->edf", slot_rows, gate_delta, preferred_element_type=jnp.float32
    ).astype(jnp.bfloat16)
    up_grad = jnp.einsum(
        "erd,erf->edf", slot_rows, up_delta, preferred_element_type=jnp.float32
    ).astype(jnp.bfloat16)
    input_part = jnp.einsum(
        "erf,edf->erd", gate_delta, gate_proj, preferred_element_type=jnp.float32
    )
    input_part = input_part + jnp.einsum(
        "erf,edf->erd", up_delta, up_proj, preferred_element_type=jnp.float32
    )
    mix_gate = jnp.dot(whole_rows, shared_gate, preferred_element_type=jnp.float32)
    mix_up = jnp.dot(whole_rows, shared_up, preferred_element_type=jnp.float32)
    mix_act, mix_slope = silu_parts(mix_gate)
    mix_hidden = (mix_act * mix_up).astype(jnp.bfloat16)
    mix_back = jnp.dot(whole_cot, shared_down, preferred_element_type=jnp.float32)
    mixgrad_gate = (mix_back * mix_up * mix_slope).astype(jnp.bfloat16)
    mixgrad_up = (mix_back * mix_act).astype(jnp.bfloat16)
    mix_partial = contract_cols(mixgrad_gate, shared_gate) + contract_cols(mixgrad_up, shared_up)
    product_cols = jnp.broadcast_to(by_peer(product), (groups * per_peer, halves))
    slot_sum, mix_sum, product_sum = (
        *side_by_side_2(
            (
                rounded(by_peer(input_part)).astype(jnp.bfloat16),
                rounded(mix_partial).astype(jnp.bfloat16),
            ),
            "tp",
            1,
            0,
        ),
        sum_at_owner(rounded(product_cols).astype(jnp.bfloat16), "tp", 1),
    )
    back_rows = slot_sum.astype(jnp.bfloat16).reshape(groups, per_peer, -1)
    back_prod = product_sum.astype(jnp.bfloat16).reshape(groups, per_peer)
    home_rows, home_prod = in_one_piece((back_rows, back_prod), EP, 0, 0, 2)
    per_slot = home_rows.reshape(experts * capacity, -1)[slot_of].astype(jnp.float32)
    token_grad = (mix_sum + jnp.sum(per_slot.reshape(token_rows, top, -1), axis=1)).astype(
        jnp.bfloat16
    )
    slot_product = home_prod.reshape(experts * capacity)[slot_of].astype(jnp.float32)
    weight_grad = slot_product.reshape(token_rows, top) / route_weights
    mix_cols = mixgrad_gate.shape[1]
    stacked = own_rows(
        jnp.concatenate(
            [
                contract_rows(whole_rows, mixgrad_gate),
                contract_rows(whole_rows, mixgrad_up),
                contract_rows(whole_cot, mix_hidden),
            ],
            axis=1,
        ),
        EP,
    )
    return (
        token_grad,
        weight_grad,
        gate_grad,
        up_grad,
        down_grad,
        stacked[:, :mix_cols],
        stacked[:, mix_cols : 2 * mix_cols],
        stacked[:, 2 * mix_cols :],
    )


def solution(mesh):
    split = Mesh(mesh.devices.reshape(8, 4, 4, mesh.shape["tp"]), ("ep_0", "ep_1", "ep_2", "tp"))
    placed = (
        P(EP, "tp"),
        P(EP, "tp"),
        P(EP, None),
        P(EP, None),
        P(EP, None, "tp"),
        P(EP, None, "tp"),
        P(EP, "tp", None),
        P(None, "tp"),
        P(None, "tp"),
        P(None, "tp"),
    )
    return jax.shard_map(
        per_device,
        mesh=split,
        in_specs=placed,
        out_specs=(
            P(EP, "tp"),
            P(EP, None),
            P(EP, None, "tp"),
            P(EP, None, "tp"),
            P(EP, "tp", None),
            P(EP, "tp"),
            P(EP, "tp"),
            P(EP, "tp"),
        ),
        check_vma=False,
    )
```

profile of v0, /device:TPU:8, one launch (start us, length us, event | category | flops | bytes accessed | tf_op | source)
XLA Modules:
  0.0 264.5 jit_solution(5470895236096575299)
XLA Ops:
  7.2 0.9 copy.47
  9.9 1.4 scatter_custom_fusion
  11.4 0.8 copy.51
  12.3 2.8 %gather_fusion.1 = f32[384]{0:T(512)S(1)} fusion(f32[256]{0:T(256)S(1)} %reshape.176, s32[1024]{0:T(1024)S(1)} %get-tuple-element.57), kind=kCustom, calls=%fused_computation.1 | custom fusion | bytes 4608 | tf_op jit(solution)/shard_map/gather | solution.py:126
  16.0 2.1 gather_fusion
  18.6 0.9 mul.87
  19.5 2.2 gather_fusion.2
  21.7 1.8 reshape.186
  24.0 1.0 copy-done.3
  25.5 2.4 pad_maximum_fusion.1
  27.9 15.8 %all-to-all-start = ((bf16[128,6,1024]{2,1,0:T(8,128)(2,1)}), bf16[128,6,1024]{2,1,0:T(8,128)(2,1)}, u32[]{:S(2)}, u32[]{:S(2)}) async-start(bf16[128,6,1024]{2,1,0:T(8,128)(2,1)} %pad_maximum_fusion.1), calls=%async_computation | async-start | bytes 4194304 | tf_op jit(solution)/shard_map/all_to_all | solution.py:22
  43.8 0.8 pad_maximum_fusion.5
  44.7 51.2 %all-to-all-done = bf16[128,6,1024]{2,1,0:T(8,128)(2,1)} async-done(((bf16[128,6,1024]{2,1,0:T(8,128)(2,1)}), bf16[128,6,1024]{2,1,0:T(8,128)(2,1)}, u32[]{:S(2)}, u32[]{:S(2)}) %all-to-all-start) | async-done | bytes 1572896 | tf_op jit(solution)/shard_map/all_to_all | solution.py:22
  95.9 3.3 %fusion.43 = (bf16[128,3,1024]{2,1,0:T(4,128)(2,1)S(1)}, bf16[128,3,1024]{2,1,0:T(4,128)(2,1)S(1)}) fusion(bf16[128,6,1024]{2,1,0:T(8,128)(2,1)} %all-to-all-done), kind=kLoop, calls=%fused_computation.92 | loop fusion | bytes 3145728 | tf_op jit(solution)/shard_map/split | solution.py:23
  99.2 2.7 %pad_maximum_fusion.2 = bf16[256,3,1024]{2,1,0:T(4,128)(2,1)} fusion(bf16[128,3,1024]{2,1,0:T(4,128)(2,1)S(1)} %get-tuple-element.45, bf16[128,3,1024]{2,1,0:T(4,128)(2,1)S(1)} %get-tuple-element.44), kind=kLoop, calls=%fused_computation.19 | loop fusion | flops 786432 | bytes 3145728 | tf_op jit(solution)/shard_map/concatenate | solution.py:14
  102.2 0.9 copy-done.7
  103.1 1.5 fusion.23
  104.6 1.3 fusion.25
  107.9 3.6 %pad_maximum_fusion = f32[2048,768]{0,1:T(8,128)} fusion(f32[2048,256]{0,1:T(8,128)S(1)} %fusion.14, f32[2048,256]{0,1:T(8,128)S(1)} %fusion.19, f32[2048,256]{0,1:T(8,128)S(1)} %fusion.21), kind=kLoop, calls=%fused_computation.6 | loop fusion | flops 3145728 | bytes 12582912 | tf_op jit(solution)/shard_map/concatenate | solution.py:206
  112.3 1.3 fusion.3
  113.6 2.3 all-gather.3.cloned.1.call-done
  115.9 4.6 %fusion.42 = (bf16[128,3,2048]{2,1,0:T(4,128)(2,1)}, bf16[128,3,2048]{2,1,0:T(4,128)(2,1)S(1)}) fusion(bf16[256,3,2048]{2,1,0:T(4,128)(2,1)} %all-gather.3.cloned.1.call-done), kind=kLoop, calls=%fused_computation.91 | loop fusion | bytes 6291456 | tf_op jit(solution)/shard_map/split | solution.py:16
  120.5 2.6 reshape.177
  123.1 3.9 %reshape.179 = bf16[384,2048]{1,0:T(8,128)(2,1)S(1)} reshape(bf16[128,3,2048]{2,1,0:T(4,128)(2,1)} %get-tuple-element.42) | data formatting | bytes 3145728 | tf_op jit(solution)/shard_map/reshape.6
  127.0 2.5 fusion.11
  129.5 0.8 fusion.9
  130.3 1.6 multiply_convert_fusion.2
  134.2 5.4 %all_to_all.20 = bf16[2,512,1024]{2,1,0:T(8,128)(2,1)S(1)} all-to-all(bf16[2,512,1024]{2,1,0:T(8,128)(2,1)S(1)} %bitcast.73), channel_id=1, replica_groups=mesh['ep_0'=8,'ep_1'=4,'ep_2'=4,'tp'=2] {'tp'}, dimensions={0} | all-to-all | bytes 4194304 | tf_op jit(solution)/shard_map/all_to_all | solution.py:34
  140.0 1.3 copy-done.5
  141.5 1.3 reshape.183
  144.1 3.7 %all_to_all.21 = bf16[2,2,192]{2,1,0:T(2,128)(2,1)S(1)} all-to-all(bf16[2,2,192]{2,1,0:T(2,128)(2,1)S(1)} %reshape.247), channel_id=1, replica_groups=mesh['ep_0'=8,'ep_1'=4,'ep_2'=4,'tp'=2] {'tp'}, dimensions={0} | all-to-all | bytes 3072 | tf_op jit(solution)/shard_map/all_to_all | solution.py:34
  148.1 46.8 %reduce-scatter.8.cloned.1.call-done = f32[256,768]{0,1:T(8,128)} async-done(((f32[2048,768]{0,1:T(8,128)}), f32[256,768]{0,1:T(8,128)}) %reduce-scatter.8.cloned.1.call-update) | async-done | bytes 786448 | tf_op jit(solution)/shard_map/reduce_scatter | solution.py:61
  195.0 2.3 copy.60
  197.3 2.8 %pad_maximum_fusion.4 = bf16[128,3,1025]{2,1,0:T(4,128)(2,1)} fusion(bf16[128,3,1]{2,1,0:T(4,128)(2,1)S(1)} %reshape_reshape.8, bf16[128,3,1024]{2,1,0:T(4,128)(2,1)} %reshape.183), kind=kLoop, calls=%fused_computation.23 | loop fusion | flops 1574400 | bytes 1574400 | tf_op jit(solution)/shard_map/concatenate | solution.py:49
  200.1 11.6 %all-to-all-start.3 = ((bf16[128,3,1025]{2,1,0:T(4,128)(2,1)}), bf16[128,3,1025]{2,1,0:T(4,128)(2,1)}, u32[]{:S(2)}, u32[]{:S(2)}) async-start(bf16[128,3,1025]{2,1,0:T(4,128)(2,1)} %pad_maximum_fusion.4), calls=%async_computation.3 | async-start | bytes 2359296 | tf_op jit(solution)/shard_map/all_to_all | solution.py:52
  211.9 1.7 fusion
  213.6 1.7 fusion.2
  215.3 6.5 %reduce-scatter.10.cloned.1.call-done = f32[64,768]{1,0:T(8,128)} async-done(((f32[256,768]{1,0:T(8,128)}), f32[64,768]{1,0:T(8,128)}) %reduce-scatter.10.cloned.1.call-update) | async-done | bytes 196624
  221.8 1.7 fusion.1
  223.5 21.7 %all-to-all-done.3 = bf16[128,3,1025]{2,1,0:T(4,128)(2,1)} async-done(((bf16[128,3,1025]{2,1,0:T(4,128)(2,1)}), bf16[128,3,1025]{2,1,0:T(4,128)(2,1)}, u32[]{:S(2)}, u32[]{:S(2)}) %all-to-all-start.3) | async-done | bytes 787232 | tf_op jit(solution)/shard_map/all_to_all | solution.py:52
  245.3 1.6 split.38
  246.8 0.7 reshape.185
  247.5 1.2 gather_fusion.3
  249.4 1.1 slice_reduce_fusion
  250.7 1.9 gather_fusion.4
  253.5 1.3 reduce_sum.55
  254.7 1.8 fusion.13
  256.6 1.4 fusion.44
  (106 shorter events, 13.6 us)
Async XLA Ops:
  7.2 123.2 %copy-start = (bf16[1,2048,256]{2,1,0:T(8,128)(2,1)S(1)}, bf16[1,2048,256]{2,1,0:T(8,128)(2,1)}, u32[]{:S(2)}) copy-start(bf16[1,2048,256]{2,1,0:T(8,128)(2,1)} %param.14) | copy-start | bytes 3145732
  7.2 8.8 %copy-start.2 = (bf16[128,1024]{1,0:T(8,128)(2,1)S(1)}, bf16[128,1024]{1,0:T(8,128)(2,1)}, u32[]{:S(2)}) copy-start(bf16[128,1024]{1,0:T(8,128)(2,1)} %param.10) | copy-start | bytes 786436
  9.9 1.4 copy-start.20
  12.3 5.7 %copy-start.19 = (s32[1024]{0:T(1024)}, s32[1024]{0:T(1024)S(1)}, u32[]{:S(2)}) copy-start(s32[1024]{0:T(1024)S(1)} %get-tuple-element.58) | copy-start | bytes 12292
  18.1 1.4 copy-start.1
  23.5 1.6 copy-start.3
  27.9 68.0 %all-to-all-start = ((bf16[128,6,1024]{2,1,0:T(8,128)(2,1)}), bf16[128,6,1024]{2,1,0:T(8,128)(2,1)}, u32[]{:S(2)}, u32[]{:S(2)}) async-start(bf16[128,6,1024]{2,1,0:T(8,128)(2,1)} %pad_maximum_fusion.1), calls=%async_computation | async-start | bytes 4194304 | tf_op jit(solution)/shard_map/all_to_all | solution.py:22
  43.7 58.5 %all-gather.5.cloned.1.call-start = ((), (), s32[]{:S(2)}) async-start(), calls=%async_computation.8 | async-start | bytes 1572864 | tf_op jit(solution)/shard_map/all_gather | solution.py:15
  44.6 71.3 %all-gather.3.cloned.1.call-start = ((), (), s32[]{:S(2)}) async-start(), calls=%async_computation.7 | async-start | bytes 6291456 | tf_op jit(solution)/shard_map/all_gather | solution.py:15
  101.9 1.2 copy-start.7
  101.9 2.7 %copy-start.8 = (bf16[2048,256]{1,0:T(8,128)(2,1)S(1)}, bf16[2048,256]{1,0:T(8,128)(2,1)}, u32[]{:S(2)}) copy-start(bf16[2048,256]{1,0:T(8,128)(2,1)} %param.18) | copy-start | bytes 3145732
  101.9 93.1 %reduce-scatter.8.cloned.1.call-start = ((), (), s32[]{:S(2)}) async-start(), calls=%async_computation.9 | async-start | bytes 7077888 | tf_op jit(solution)/shard_map/reduce_scatter | solution.py:61
  103.1 2.9 %copy-start.4 = (bf16[256,2048]{1,0:T(8,128)(2,1)S(1)}, bf16[256,2048]{1,0:T(8,128)(2,1)}, u32[]{:S(2)}) copy-start(bf16[256,2048]{1,0:T(8,128)(2,1)} %all-gather.5.cloned.1.call-done) | copy-start | bytes 3145732
  103.1 2.9 %copy-start.22 = (bf16[2048,256]{1,0:T(8,128)(2,1)S(1)}, bf16[2048,256]{1,0:T(8,128)(2,1)}, u32[]{:S(2)}) copy-start(bf16[2048,256]{1,0:T(8,128)(2,1)} %param.19) | copy-start | bytes 3145732
  106.3 0.6 copy-start.17
  111.5 0.8 copy-start.18
  111.5 110.3 %reduce-scatter.10.cloned.1.call-start = ((), (), s32[]{:S(2)}) async-start(), calls=%async_computation.10 | async-start | bytes 983040
  127.0 2.5 copy-start.6
  130.3 1.6 copy-start.15
  131.9 0.7 copy-start.13
  131.9 0.7 copy-start.11
  132.7 1.0 copy-start.9
  140.0 1.3 copy-start.5
  197.3 14.6 %copy-start.21 = (s32[256,1]{0,1:T(1,128)S(1)}, s32[256,1]{0,1:T(1,128)}, u32[]{:S(2)}) copy-start(s32[256,1]{0,1:T(1,128)} %copy-done.20) | copy-start | bytes 3076
  197.3 14.6 %copy-start.14 = (bf16[384,256]{0,1:T(8,128)(2,1)S(1)}, bf16[384,256]{0,1:T(8,128)(2,1)}, u32[]{:S(2)}) copy-start(bf16[384,256]{0,1:T(8,128)(2,1)} %copy-done.13) | copy-start | bytes 589828
  200.1 13.5 %copy-start.16 = (f32[384,256]{0,1:T(8,128)S(1)}, f32[384,256]{0,1:T(8,128)}, u32[]{:S(2)}) copy-start(f32[384,256]{0,1:T(8,128)} %copy-done.15) | copy-start | bytes 1179652
  200.1 45.1 %all-to-all-start.3 = ((bf16[128,3,1025]{2,1,0:T(4,128)(2,1)}), bf16[128,3,1025]{2,1,0:T(4,128)(2,1)}, u32[]{:S(2)}, u32[]{:S(2)}) async-start(bf16[128,3,1025]{2,1,0:T(4,128)(2,1)} %pad_maximum_fusion.4), calls=%async_computation.3 | async-start | bytes 2359296 | tf_op jit(solution)/shard_map/all_to_all | solution.py:52
  211.8 44.8 %reduce-scatter.12.cloned.1.call-start = ((), (), s32[]{:S(2)}) async-start(), calls=%async_computation.11 | async-start | bytes 245760
  211.8 1.8 copy-start.10
  211.8 1.8 copy-start.23
  213.6 8.2 %copy-start.12 = (bf16[384,256]{0,1:T(8,128)(2,1)S(1)}, bf16[384,256]{0,1:T(8,128)(2,1)}, u32[]{:S(2)}) copy-start(bf16[384,256]{0,1:T(8,128)(2,1)} %copy-done.11) | copy-start | bytes 589828
Sparse Core Ops, SparseCore 0:
  46.9 15.6 all-gather.4
  102.0 13.8 all-gather.2
  118.5 76.4 reduce-scatter.7
  198.0 23.7 reduce-scatter.9
  224.1 27.0 reduce-scatter.11
where the time goes:
time: 265 us; the launch traced here: 264 us
  waiting for transfers between devices  129 us (49%)
  local copies, waits for them, and re-layouts  47.4 us (18%)
  starting transfers between devices  27.8 us (10%)
  other arithmetic  19.5 us (7%)
  matrix products  17.6 us (7%)
  between operations  14.3 us (5%)
  blocking collectives  9.1 us (3%)
    all_to_all x1, waiting for transfers between devices, side_by_side(): lax.all_to_all(both, axis, split_axis=split_dim, concat_axis=concat_dim,...  51.2 us
    reduce_scatter x1, waiting for transfers between devices, own_rows(): running = lax.psum_scatter(running, axis, scatter_dimension=0, tiled=True)  46.8 us
    all_to_all x1, waiting for transfers between devices, in_one_piece(): lax.all_to_all(both, axis, split_axis=split_dim, concat_axis=concat_dim,...  21.7 us
    all_to_all x1, starting transfers between devices, side_by_side(): lax.all_to_all(both, axis, split_axis=split_dim, concat_axis=concat_dim,...  15.8 us
    all_to_all x1, starting transfers between devices, in_one_piece(): lax.all_to_all(both, axis, split_axis=split_dim, concat_axis=concat_dim,...  11.6 us
    unnamed x56, local copies, waits for them, and re-layouts  9.64 us
    all_to_all x2, blocking collectives, sum_at_owner(): blocks = lax.all_to_all(split_up(shard, dim, peers), axis, 0, 0, tiled=True)  9.1 us
    unnamed x7, waiting for transfers between devices  6.55 us
  transfers between devices with their start and end apart: 7, of which 5 were waited for; matrix products, arithmetic and copies ran while one was open for 22% of the time, Pallas kernels for 0%

commit v1 on v0

--- a/solution.py
+++ b/solution.py
@@ -3,6 +3,8 @@
 import jax
 import jax.numpy as jnp
 from jax import lax
+from jax.experimental import pallas as pl
+from jax.experimental.pallas import tpu as pltpu
 from jax.sharding import Mesh
 from jax.sharding import PartitionSpec as P
 
@@ -13,13 +15,6 @@
     widths = [a.shape[along] for a in arrays]
     both = jnp.concatenate(arrays, axis=along)
     filled = lax.all_gather(both, axis, axis=dim, tiled=True)
-    return tuple(jnp.split(filled, [sum(widths[:k]) for k in range(1, len(widths))], axis=along))
-
-
-def side_by_side(arrays, axis, split_dim, concat_dim, along):
-    widths = [a.shape[along] for a in arrays]
-    both = jnp.concatenate(arrays, axis=along)
-    filled = lax.all_to_all(both, axis, split_axis=split_dim, concat_axis=concat_dim, tiled=True)
     return tuple(jnp.split(filled, [sum(widths[:k]) for k in range(1, len(widths))], axis=along))
 
 
@@ -44,22 +39,71 @@
     return tuple(outs)
 
 
-def in_one_piece(arrays, axis, split_dim, concat_dim, along):
-    widths = [math.prod(a.shape[along:]) for a in arrays]
-    both = jnp.concatenate(
-        [a.reshape(*a.shape[:along], w) for a, w in zip(arrays, widths)], axis=along
-    )
-    filled = lax.all_to_all(both, axis, split_axis=split_dim, concat_axis=concat_dim, tiled=True)
-    blocks = jnp.split(filled, [sum(widths[:k]) for k in range(1, len(widths))], axis=along)
-    return tuple(
-        (b.reshape(*filled.shape[:along], *a.shape[along:]) for a, b in zip(arrays, blocks))
-    )
+def direct_kernel(send, recv, send_sem, recv_sem):
+    z, y, x, c = (lax.axis_index(n) for n in ("ep_0", "ep_1", "ep_2", "tp"))
+    nz, ny, nx = (lax.axis_size(n) for n in ("ep_0", "ep_1", "ep_2"))
+    count = nz * ny * nx
+    me = (z * ny + y) * nx + x
+
+    def peer(step):
+        pz = lax.rem(z + step // (ny * nx), nz)
+        py = lax.rem(y + lax.rem(step // nx, ny), ny)
+        px = lax.rem(x + lax.rem(step, nx), nx)
+        return (pz * ny + py) * nx + px, (pz, py, px, c)
+
+    barrier = pltpu.get_barrier_semaphore()
+
+    def greet(step, carry):
+        pl.semaphore_signal(
+            barrier, inc=1, device_id=peer(step)[1], device_id_type=pl.DeviceIdType.MESH
+        )
+        return carry
+
+    lax.fori_loop(1, count, greet, 0)
+    recv[me] = send[me]
+    pl.semaphore_wait(barrier, count - 1)
+
+    def launch(step, carry):
+        index, device = peer(step)
+        pltpu.make_async_remote_copy(
+            src_ref=send.at[index],
+            dst_ref=recv.at[me],
+            send_sem=send_sem,
+            recv_sem=recv_sem,
+            device_id=device,
+            device_id_type=pl.DeviceIdType.MESH,
+        ).start()
+        return carry
+
+    lax.fori_loop(1, count, launch, 0)
+    rest = pl.ds(0, count - 1)
+    pltpu.make_async_copy(send.at[rest], send.at[rest], send_sem).wait()
+    pltpu.make_async_copy(recv.at[rest], recv.at[rest], recv_sem).wait()
+
+
+def direct_exchange(blocks, collective_id):
+    return pl.pallas_call(
+        direct_kernel,
+        out_shape=jax.ShapeDtypeStruct(blocks.shape, blocks.dtype),
+        in_specs=[pl.BlockSpec(memory_space=pltpu.VMEM)],
+        out_specs=pl.BlockSpec(memory_space=pltpu.VMEM),
+        scratch_shapes=[pltpu.SemaphoreType.DMA, pltpu.SemaphoreType.DMA],
+        compiler_params=pltpu.CompilerParams(
+            collective_id=collective_id, has_side_effects=True, vmem_limit_bytes=16 << 20
+        ),
+        name=f"direct_{collective_id}",
+    )(blocks)
 
 
 def own_rows(running, axes):
-    for axis in axes:
+    sizes = [lax.axis_size(axis) for axis in axes]
+    total = math.prod(sizes)
+    rows, cols = running.shape
+    blocks = running.astype(jnp.bfloat16).reshape(*sizes, rows // total, cols)
+    running = blocks.transpose(2, 1, 0, 3, 4).reshape(rows, cols)
+    for axis in axes[::-1]:
         running = lax.psum_scatter(running, axis, scatter_dimension=0, tiled=True)
-    return running
+    return running.astype(jnp.float32)
 
 
 def slot_table(routes, experts, capacity):
@@ -132,7 +176,10 @@
     )
     sent_rows = packed_rows.reshape(groups, per_peer, col_count)
     sent_cot = packed_cot.reshape(groups, per_peer, col_count)
-    half_rows, half_cot = side_by_side((sent_rows, sent_cot), EP, 0, 0, 1)
+    both = jnp.concatenate((sent_rows, sent_cot), axis=1)
+    arrived = direct_exchange(both.reshape(groups, -1, 128), 0)
+    arrived = arrived.reshape(groups, 2 * per_peer, col_count)
+    half_rows, half_cot = arrived[:, :per_peer], arrived[:, per_peer:]
     got_rows, got_cot = sent_together((half_rows, half_cot), "tp", 2, 0)
 
     def by_expert(layout):
@@ -194,7 +241,11 @@
     )
     back_rows = slot_sum.astype(jnp.bfloat16).reshape(groups, per_peer, -1)
     back_prod = product_sum.astype(jnp.bfloat16).reshape(groups, per_peer)
-    home_rows, home_prod = in_one_piece((back_rows, back_prod), EP, 0, 0, 2)
+    tail = jnp.pad(back_prod[:, None, :], ((0, 0), (0, 7), (0, 128 - per_peer)))
+    leaving = jnp.concatenate((back_rows.reshape(groups, -1, 128), tail), axis=1)
+    home = direct_exchange(leaving, 1)
+    home_rows = home[:, : per_peer * 8].reshape(groups, per_peer, -1)
+    home_prod = home[:, per_peer * 8, :per_peer]
     per_slot = home_rows.reshape(experts * capacity, -1)[slot_of].astype(jnp.float32)
     token_grad = (mix_sum + jnp.sum(per_slot.reshape(token_rows, top, -1), axis=1)).astype(
         jnp.bfloat16

time: 265 us -> 261 us (0.985)
  Pallas kernels: 0 us -> 88.2 us
  waiting for transfers between devices: 129 us -> 50.4 us
  starting transfers between devices: 27.8 us -> 0.38 us
  local copies, waits for them, and re-layouts: 47.4 us -> 60 us
  other arithmetic: 19.5 us -> 15.9 us
  matrix products: 17.6 us -> 21.1 us
    pallas_call x0 -> x2, Pallas kernels: none -> 88.2 us  [direct_exchange(): pl.pallas_call(direct_kernel, out_shape=jax.ShapeDtypeStruct(blocks.shape...]
    all_to_all x2 -> x0, waiting for transfers between devices: 73 us -> none  [the longest x1 51.2 us: side_by_side(): lax.all_to_all(both, axis, split_axis=split_dim, concat_axis=concat_dim,...]
    all_to_all x2 -> x0, starting transfers between devices: 27.4 us -> none  [the longest x1 15.8 us: side_by_side(): lax.all_to_all(both, axis, split_axis=split_dim, concat_axis=concat_dim,...]
    unnamed x7 -> x5, waiting for transfers between devices: 6.55 us -> 0.08 us
    concatenate x3 -> x2, other arithmetic: 8.79 us -> 2.39 us  [the longest x1 1.3 us: per_device(): jnp.concatenate((back_rows.reshape(groups, -1, 128), tail), axis=1)]
    split x1 -> x3, local copies, waits for them, and re-layouts: 4.6 us -> 10.7 us  [sent_together(): jnp.split(filled, [sum(widths[:k]) for k in range(1, len(widths))], axis=...]
    split x3 -> x0, local copies, waits for them, and re-layouts: 6.01 us -> none  [the longest x1 3.3 us: side_by_side(): jnp.split(filled, [sum(widths[:k]) for k in range(1, len(widths))], axis=...]
    another operation x6 -> x8, local copies, waits for them, and re-layouts: 6.75 us -> 11.9 us
  transfers between devices with their start and end apart: 7 -> 5, of which waited for: 5 -> 3; matrix products, arithmetic and copies ran while one was open for 22% -> 35% of each run, Pallas kernels for 0% -> 34%
where the time goes in v1:
time: 261 us; the launch traced here: 260 us
  Pallas kernels  88.2 us (34%)
  local copies, waits for them, and re-layouts  60 us (23%)
  waiting for transfers between devices  50.4 us (19%)
  matrix products  21.1 us (8%)
  other arithmetic  15.9 us (6%)
  between operations  14.4 us (6%)
  blocking collectives  9.1 us (3%)
    pallas_call x2, Pallas kernels, direct_exchange(): pl.pallas_call(direct_kernel, out_shape=jax.ShapeDtypeStruct(blocks.shape...  88.2 us
    reduce_scatter x3, waiting for transfers between devices, own_rows(): running = lax.psum_scatter(running, axis, scatter_dimension=0, tiled=True)  44.1 us
    split x3, local copies, waits for them, and re-layouts, sent_together(): jnp.split(filled, [sum(widths[:k]) for k in range(1, len(widths))], axis=...  10.7 us
    all_to_all x2, blocking collectives, sum_at_owner(): blocks = lax.all_to_all(split_up(shard, dim, peers), axis, 0, 0, tiled=True)  9.1 us
    another operation x5, local copies, waits for them, and re-layouts  9.06 us
    all_gather x2, waiting for transfers between devices, sent_together(): filled = lax.all_gather(both, axis, axis=dim, tiled=True)  6.22 us
  transfers between devices with their start and end apart: 5, of which 3 were waited for; matrix products, arithmetic and copies ran while one was open for 35% of the time, Pallas kernels for 34%

profile of v1, /device:TPU:8, one launch (start us, length us, event | category | flops | bytes accessed | tf_op | source)
XLA Modules:
  0.0 259.5 jit_solution(5985722346412117249)
XLA Ops:
  7.2 2.0 pad_maximum_fusion.3
  11.9 1.4 scatter_custom_fusion
  13.4 2.7 %gather_fusion.2 = bf16[384,1024]{1,0:T(8,128)(2,1)} fusion(bf16[128,1024]{1,0:T(8,128)(2,1)S(1)} %copy-done.2, s32[1024]{0:T(1024)S(1)} %get-tuple-element.50), kind=kCustom, calls=%fused_computation.2 | custom fusion | bytes 1574400 | tf_op jit(solution)/shard_map/gather | solution.py:174
  16.1 2.1 gather_fusion
  18.4 2.8 %gather_fusion.1 = f32[384]{0:T(512)S(1)} fusion(f32[256]{0:T(256)S(1)} %reshape.186, s32[1024]{0:T(1024)S(1)} %get-tuple-element.49), kind=kCustom, calls=%fused_computation.1 | custom fusion | bytes 4608 | tf_op jit(solution)/shard_map/gather | solution.py:170
  21.7 1.3 gather.18
  23.0 2.5 reshape.197
  25.4 1.8 broadcast_select_fusion
  27.7 1.1 pad_maximum_fusion
  28.8 2.6 %copy.56 = bf16[128,6,1024]{0,2,1:T(8,128)(2,1)} copy(bf16[128,6,1024]{2,1,0:T(8,128)(2,1)S(1)} %pad_maximum_fusion) | data formatting | bytes 3145728 | tf_op jit(solution)/shard_map/concatenate | solution.py:179
  31.4 2.0 copy.57.send
  33.5 50.6 %direct_0.1 = bf16[128,48,128]{2,1,0:T(8,128)(2,1)S(1)} custom-call(bf16[128,48,128]{2,1,0:T(8,128)(2,1)S(1)} %copy.57.send), custom_call_target="tpu_custom_call" | custom-call | tf_op jit(solution)/shard_map/direct_0/pallas_call | solution.py:85
  84.1 1.1 copy-done.1
  85.2 2.1 copy.58
  87.5 1.3 pad_maximum_fusion.2
  89.0 1.5 fusion.22
  90.5 1.3 fusion.24
  93.9 2.0 copy.65
  96.7 1.3 fusion.3
  98.0 6.2 %all-gather.3.cloned.1.call-done = bf16[256,3,2048]{0,2,1:T(8,128)(2,1)} async-done(((bf16[256,3,1024]{0,2,1:T(8,128)(2,1)}), bf16[256,3,2048]{0,2,1:T(8,128)(2,1)}) %all-gather.3.cloned.1.call-update) | async-done | bytes 3145744 | tf_op jit(solution)/shard_map/all_gather | solution.py:17
  104.2 3.2 %fusion.41 = (bf16[128,3,2048]{0,2,1:T(8,128)(2,1)S(1)}, bf16[128,3,2048]{0,2,1:T(8,128)(2,1)}) fusion(bf16[256,3,2048]{0,2,1:T(8,128)(2,1)} %all-gather.3.cloned.1.call-done), kind=kLoop, calls=%fused_computation.93 | loop fusion | bytes 6291456 | tf_op jit(solution)/shard_map/split | solution.py:18
  107.4 3.0 %copy.60 = bf16[128,3,2048]{2,1,0:T(4,128)(2,1)} copy(bf16[128,3,2048]{0,2,1:T(8,128)(2,1)S(1)} %get-tuple-element.34) | data formatting | bytes 3145728 | tf_op jit(solution)/shard_map/split | solution.py:18
  110.3 3.9 %reshape.191 = bf16[384,2048]{1,0:T(8,128)(2,1)S(1)} reshape(bf16[128,3,2048]{2,1,0:T(4,128)(2,1)} %copy.60) | data formatting | bytes 3145728 | tf_op jit(solution)/shard_map/reshape.6
  114.3 4.5 %copy.59 = bf16[128,3,2048]{2,1,0:T(4,128)(2,1)} copy(bf16[128,3,2048]{0,2,1:T(8,128)(2,1)} %get-tuple-element.35) | data formatting | bytes 3145728 | tf_op jit(solution)/shard_map/split | solution.py:18
  118.8 5.1 %reshape.189 = bf16[384,2048]{1,0:T(8,128)(2,1)} reshape(bf16[128,3,2048]{2,1,0:T(4,128)(2,1)} %copy.59) | data formatting | bytes 3145728 | tf_op jit(solution)/shard_map/reshape.3
  123.9 2.1 fusion.11
  126.8 1.6 multiply_convert_fusion.2
  129.8 3.7 %all_to_all.10 = bf16[2,2,192]{2,1,0:T(2,128)(2,1)S(1)} all-to-all(bf16[2,2,192]{2,1,0:T(2,128)(2,1)S(1)} %reshape.254), channel_id=1, replica_groups=mesh['ep_0'=8,'ep_1'=4,'ep_2'=4,'tp'=2] {'tp'}, dimensions={0} | all-to-all | bytes 3072 | tf_op jit(solution)/shard_map/all_to_all | solution.py:29
  133.8 2.3 fusion.6
  136.1 12.7 %reduce-scatter.4.cloned.1.call-done = bf16[512,768]{1,0:T(8,128)(2,1)} async-done(((bf16[2048,768]{1,0:T(8,128)(2,1)}), bf16[512,768]{1,0:T(8,128)(2,1)}) %reduce-scatter.4.cloned.1.call-update) | async-done | bytes 786448 | tf_op jit(solution)/shard_map/reduce_scatter | solution.py:105
  148.9 2.9 %add_convert_fusion = bf16[384,2048]{1,0:T(8,128)(2,1)S(1)} fusion(f32[384,2048]{1,0:T(8,128)} %fusion.6, bf16[384,256]{0,1:T(8,128)(2,1)S(1)} %get-tuple-element.40, bf16[1,2048,256]{2,1,0:T(8,128)(2,1)} %param.15), kind=kOutput, calls=%fused_computation.8 | convolution fusion | flops 404226048 | bytes 5963776 | tf_op jit(solution)/shard_map/erf,edf->erd/dot_general | solution.py:218
  152.3 5.4 %all_to_all.11 = bf16[2,512,1024]{2,1,0:T(8,128)(2,1)S(1)} all-to-all(bf16[2,512,1024]{2,1,0:T(8,128)(2,1)S(1)} %bitcast.81), channel_id=1, replica_groups=mesh['ep_0'=8,'ep_1'=4,'ep_2'=4,'tp'=2] {'tp'}, dimensions={0} | all-to-all | bytes 4194304 | tf_op jit(solution)/shard_map/all_to_all | solution.py:29
  158.2 1.3 copy-done.5
  159.6 1.2 reshape_reshape.6
  160.8 1.3 fusion.5.send
  162.2 37.6 %direct_1.1 = bf16[128,32,128]{2,1,0:T(8,128)(2,1)S(1)} custom-call(bf16[128,32,128]{2,1,0:T(8,128)(2,1)S(1)} %fusion.5.send), custom_call_target="tpu_custom_call" | custom-call | tf_op jit(solution)/shard_map/direct_1/pallas_call | solution.py:85
  199.7 1.0 slice.40
  201.1 1.4 reshape_reshape.7
  202.5 1.9 gather_fusion.4
  204.5 2.0 gather_fusion.3
  208.1 2.7 %reshape.198 = f32[128,2,1024]{2,1,0:T(2,128)} reshape(bf16[256,1024]{1,0:T(8,128)(2,1)} %gather_fusion.3) | data formatting | bytes 1572864 | tf_op jit(solution)/shard_map/convert_element_type | solution.py:249
  210.7 2.5 reduce_sum.55
  213.2 1.7 fusion
  215.0 1.8 fusion.15
  216.8 1.7 fusion.1
  218.5 1.7 fusion.2
  220.2 31.4 %reduce-scatter.8.cloned.1.call-done = bf16[16,768]{1,0:T(8,128)(2,1)} async-done(((bf16[128,768]{1,0:T(8,128)(2,1)}), bf16[16,768]{1,0:T(8,128)(2,1)}) %reduce-scatter.8.cloned.1.call-update) | async-done | bytes 24592 | tf_op jit(solution)/shard_map/reduce_scatter | solution.py:105
  251.7 1.3 fusion.43
  (105 shorter events, 12.4 us)
Async XLA Ops:
  7.2 119.6 %copy-start = (bf16[1,2048,256]{2,1,0:T(8,128)(2,1)S(1)}, bf16[1,2048,256]{2,1,0:T(8,128)(2,1)}, u32[]{:S(2)}) copy-start(bf16[1,2048,256]{2,1,0:T(8,128)(2,1)} %param.14) | copy-start | bytes 3145732
  7.2 6.2 %copy-start.2 = (bf16[128,1024]{1,0:T(8,128)(2,1)S(1)}, bf16[128,1024]{1,0:T(8,128)(2,1)}, u32[]{:S(2)}) copy-start(bf16[128,1024]{1,0:T(8,128)(2,1)} %param.11) | copy-start | bytes 786436
  7.2 81.7 %all-gather.5.cloned.1.call-start = ((), (), s32[]{:S(2)}) async-start(), calls=%async_computation.6 | async-start | bytes 1572864 | tf_op jit(solution)/shard_map/all_gather | solution.py:17
  9.2 94.9 %all-gather.3.cloned.1.call-start = ((), (), s32[]{:S(2)}) async-start(), calls=%async_computation.5 | async-start | bytes 4718592 | tf_op jit(solution)/shard_map/all_gather | solution.py:17
  13.4 2.7 %copy-start.3 = (bf16[128,1024]{1,0:T(8,128)(2,1)S(1)}, bf16[128,1024]{1,0:T(8,128)(2,1)}, u32[]{:S(2)}) copy-start(bf16[128,1024]{1,0:T(8,128)(2,1)} %param.10) | copy-start | bytes 786436
  16.1 2.1 copy-start.18
  18.3 3.4 %copy-start.15 = (f32[128,2]{1,0:T(8,128)}, f32[128,2]{1,0:T(8,128)S(1)}, u32[]{:S(2)}) copy-start(f32[128,2]{1,0:T(8,128)S(1)} %copy.55) | copy-start | bytes 3076
  84.1 1.1 copy-start.1
  87.5 1.5 copy-start.6
  88.8 1.7 copy-start.7
  88.8 60.0 %reduce-scatter.4.cloned.1.call-start = ((), (), s32[]{:S(2)}) async-start(), calls=%async_computation.7 | async-start | bytes 3932160 | tf_op jit(solution)/shard_map/reduce_scatter | solution.py:105
  89.0 2.9 %copy-start.4 = (bf16[256,2048]{1,0:T(8,128)(2,1)S(1)}, bf16[256,2048]{1,0:T(8,128)(2,1)}, u32[]{:S(2)}) copy-start(bf16[256,2048]{1,0:T(8,128)(2,1)} %all-gather.5.cloned.1.call-done) | copy-start | bytes 3145732
  89.0 2.9 %copy-start.19 = (bf16[2048,256]{1,0:T(8,128)(2,1)S(1)}, bf16[2048,256]{1,0:T(8,128)(2,1)}, u32[]{:S(2)}) copy-start(bf16[2048,256]{1,0:T(8,128)(2,1)} %param.19) | copy-start | bytes 3145732
  96.0 120.8 %reduce-scatter.6.cloned.1.call-start = ((), (), s32[]{:S(2)}) async-start(), calls=%async_computation.8 | async-start | bytes 983040 | tf_op jit(solution)/shard_map/reduce_scatter | solution.py:105
  123.9 2.1 copy-start.9
  123.9 2.1 copy-start.20
  126.0 2.4 copy-start.16
  128.4 7.7 %copy-start.13 = (bf16[384,256]{0,1:T(8,128)(2,1)}, bf16[384,256]{0,1:T(8,128)(2,1)S(1)}, u32[]{:S(2)}) copy-start(bf16[384,256]{0,1:T(8,128)(2,1)S(1)} %get-tuple-element.38) | copy-start | bytes 589828
  128.4 20.5 %copy-start.11 = (bf16[384,256]{0,1:T(8,128)(2,1)}, bf16[384,256]{0,1:T(8,128)(2,1)S(1)}, u32[]{:S(2)}) copy-start(bf16[384,256]{0,1:T(8,128)(2,1)S(1)} %get-tuple-element.40) | copy-start | bytes 589828
  148.9 102.8 %reduce-scatter.8.cloned.1.call-start = ((), (), s32[]{:S(2)}) async-start(), calls=%async_computation.9 | async-start | bytes 221184 | tf_op jit(solution)/shard_map/reduce_scatter | solution.py:105
  148.9 2.9 %copy-start.8 = (bf16[128,2048]{1,0:T(8,128)(2,1)S(1)}, bf16[128,2048]{1,0:T(8,128)(2,1)}, u32[]{:S(2)}) copy-start(bf16[128,2048]{1,0:T(8,128)(2,1)} %fusion.3) | copy-start | bytes 1572868
  158.2 1.3 copy-start.5
  206.4 6.8 %copy-start.14 = (bf16[384,256]{0,1:T(8,128)(2,1)S(1)}, bf16[384,256]{0,1:T(8,128)(2,1)}, u32[]{:S(2)}) copy-start(bf16[384,256]{0,1:T(8,128)(2,1)} %copy-done.13) | copy-start | bytes 589828
  213.2 3.6 %copy-start.12 = (bf16[384,256]{0,1:T(8,128)(2,1)S(1)}, bf16[384,256]{0,1:T(8,128)(2,1)}, u32[]{:S(2)}) copy-start(bf16[384,256]{0,1:T(8,128)(2,1)} %copy-done.11) | copy-start | bytes 589828
  216.8 1.8 copy-start.17
  216.8 1.7 copy-start.10
  216.8 1.7 copy-start.21
Sparse Core Ops, SparseCore 0:
  10.4 17.2 all-gather.4
  88.9 15.1 all-gather.2
  106.7 42.0 reduce-scatter.3
  151.2 22.6 reduce-scatter.5
  216.9 34.7 reduce-scatter.7

commit v2 on v0

v2 whole, which is shorter than its diff:
```python
import jax
import jax.numpy as jnp
from jax import lax
from jax.experimental import pallas as pl
from jax.experimental.pallas import tpu as pltpu
from jax.sharding import Mesh
from jax.sharding import PartitionSpec as P

EP = ("ep_0", "ep_1", "ep_2")
BF = jnp.bfloat16
F32 = jnp.float32
CAP = 3
LANES = 128


def dot(left, right, dims):
    return lax.dot_general(left, right, ((dims[:1], dims[1:]), ((), ())), preferred_element_type=F32)


def silu_parts(preact):
    sigmoid_v = jax.nn.sigmoid(preact)
    return (preact * sigmoid_v, sigmoid_v * (1.0 + preact * (1.0 - sigmoid_v)))


def fused_kernel(
    nz, ny, nx,
    tokens, cotangent, routes, route_weights, gate_proj, up_proj, down_proj,
    shared_gate, shared_up, shared_down,
    token_grad, weight_grad, gate_grad, up_grad, down_grad, sgate_grad, sup_grad, sdown_grad,
    wtok, wcot, wgu, wd, sgu, sd,
    onehot, wide, wide2, send1, recv1, fwd1, rows, cots,
    pre, back, hidden, delta, part, part_in, prod, prod_in, prod_out, prod_home,
    send2, recv2, home, mix, mix_in, mix_sum, smix, shid,
    grad_gu, grad_d, ga, gb, ra1, rb1, sa2, sb2, ra2, rb2, sa3, sb3, ra3, rb3,
    load_sem, tp_send, tp_recv, s1_sem, r1_sem, f_send, f_recv, p_send, p_recv,
    m_send, m_recv, s2_sem, r2_sem, q_send, q_recv, rs_send, rs_recv, out_sem,
):
    z, y, x, c = (lax.axis_index(n) for n in EP + ("tp",))
    chips = nz * ny * nx
    plane = ny * nx
    me = (z * ny + y) * nx + x
    toks, half = tokens.shape
    width = 2 * half
    hid = wd.shape[0]
    chunks = half // LANES
    q1 = 2 * CAP * chunks
    q2 = CAP * chunks
    first = pl.ds(pl.multiple_of(c * half, LANES), half)
    second = pl.ds(pl.multiple_of((1 - c) * half, LANES), half)
    partner = (z, y, x, 1 - c)

    def remote(src, dst, send_sem, recv_sem, device):
        return pltpu.make_async_remote_copy(
            src_ref=src, dst_ref=dst, send_sem=send_sem, recv_sem=recv_sem,
            device_id=device, device_id_type=pl.DeviceIdType.MESH,
        )

    def await_bytes(ref, sem):
        pltpu.make_async_copy(ref, ref, sem).wait()

    def peer(step):
        pz = lax.rem(z + step // plane, nz)
        py = lax.rem(y + lax.rem(step // nx, ny), ny)
        px = lax.rem(x + lax.rem(step, nx), nx)
        return (pz * ny + py) * nx + px, (pz, py, px, c)

    loads = [
        pltpu.make_async_copy(src, dst, load_sem.at[i])
        for i, (src, dst) in enumerate(
            (
                (tokens, wtok.at[:, :half]),
                (cotangent, wcot.at[:, :half]),
                (shared_gate.at[first], sgu.at[:half, :hid]),
                (shared_gate.at[second], sgu.at[half:, :hid]),
                (shared_up.at[first], sgu.at[:half, hid:]),
                (shared_up.at[second], sgu.at[half:, hid:]),
                (shared_down.at[first], sd.at[:half]),
                (shared_down.at[second], sd.at[half:]),
                (gate_proj.at[first], wgu.at[:half, :hid]),
                (gate_proj.at[second], wgu.at[half:, :hid]),
                (up_proj.at[first], wgu.at[:half, hid:]),
                (up_proj.at[second], wgu.at[half:, hid:]),
                (down_proj.at[:, first], wd.at[:, :half]),
                (down_proj.at[:, second], wd.at[:, half:]),
            )
        )
    ]
    for copy in loads:
        copy.start()

    barrier = pltpu.get_barrier_semaphore()
    pl.semaphore_signal(barrier, inc=1, device_id=partner, device_id_type=pl.DeviceIdType.MESH)

    def greet(step, carry):
        pl.semaphore_signal(
            barrier, inc=1, device_id=peer(step)[1], device_id_type=pl.DeviceIdType.MESH
        )
        return carry

    lax.fori_loop(1, chips, greet, 0)

    lane = lax.broadcasted_iota(jnp.int32, (toks, chips), 1)
    sub = lax.broadcasted_iota(jnp.int32, (toks, chips), 0)
    picks = [routes[:, k : k + 1] == lane for k in range(2)]
    named = picks[0].astype(F32) + picks[1].astype(F32)
    earlier = dot((lane < sub).astype(BF), named.astype(BF), (1, 0))
    weight_of = jnp.where(picks[0], route_weights[:, 0:1], 0.0) + jnp.where(
        picks[1], route_weights[:, 1:2], 0.0
    )
    columns = []
    for r in range(CAP):
        held = jnp.where(earlier == float(r), named, 0.0)
        onehot[:, r * chips : (r + 1) * chips] = held.astype(BF)
        row = jnp.sum(held * weight_of, axis=0, keepdims=True)
        columns.append(jnp.sum(jnp.where(lane == sub, row, 0.0), axis=1, keepdims=True))

    loads[0].wait()
    loads[1].wait()
    for r in range(CAP):
        pick = onehot[:, r * chips : (r + 1) * chips]
        for t, source in enumerate((wtok, wcot)):
            chosen = dot(pick, source[:, :half], (0, 0))
            if t == 1:
                chosen = columns[r] * chosen
            for k in range(chunks):
                wide[pl.ds((t * CAP + r) * chunks + k, chips, stride=q1), :] = chosen[
                    :, k * LANES : (k + 1) * LANES
                ]

    def narrow(i, carry):
        block = wide[pl.ds(pl.multiple_of(i * plane * q1, plane * q1), plane * q1), :]
        send1[pl.ds(i * plane, plane)] = block.reshape(plane, q1, LANES).astype(BF)
        return carry

    lax.fori_loop(0, nz, narrow, 0)
    recv1[me] = send1[me]

    pl.semaphore_wait(barrier, chips)

    trade = [
        remote(ref.at[:, :half], ref.at[:, half:], tp_send.at[i], tp_recv.at[i], partner)
        for i, ref in enumerate((wtok, wcot))
    ]
    for copy in trade:
        copy.start()

    def launch(step, carry):
        index, device = peer(step)
        remote(send1.at[index], recv1.at[me], s1_sem, r1_sem.at[step // plane], device).start()
        return carry

    lax.fori_loop(1, chips, launch, 0)

    for copy in loads[2:8]:
        copy.wait()
    for copy in trade:
        copy.wait()
    smix[...] = dot(wtok[...], sgu[...], (1, 0))
    mix_back = dot(wcot[...], sd[...], (1, 0))
    mix_act, mix_slope = silu_parts(smix[:, :hid])
    mix_up = smix[:, hid:]
    shid[:, 2 * hid :] = (mix_act * mix_up).astype(BF)
    shid[:, :hid] = (mix_back * mix_up * mix_slope).astype(BF)
    shid[:, hid : 2 * hid] = (mix_back * mix_act).astype(BF)

    zrows = width // nz
    zhalf = nz // 2
    cut = ga.shape[-1]

    def shared_terms(i, carry):
        at = pl.ds(pl.multiple_of(i * zrows, LANES), zrows)
        block = lax.rem(i + c * zhalf, nz)
        one = dot(wtok[:, at], shid[:, : 2 * hid], (0, 0)).astype(BF)
        two = dot(wcot[:, at], shid[:, 2 * hid :], (0, 0)).astype(BF)
        ga[block] = one[:, :cut].reshape(ny, nx, zrows // plane, cut)
        gb[block, :, :, :, : 2 * hid - cut] = one[:, cut:].reshape(
            ny, nx, zrows // plane, 2 * hid - cut
        )
        gb[block, :, :, :, 2 * hid - cut :] = two.reshape(ny, nx, zrows // plane, hid)
        return carry

    lax.fori_loop(0, nz, shared_terms, 0)

    mix[...] = dot(shid[:, : 2 * hid], sgu[half:, :], (1, 1)).astype(BF)
    trade_mix = remote(mix, mix_in, m_send, m_recv, partner)
    trade_mix.start()
    for d in range(1, nx):
        px = lax.rem(x + d, nx)
        remote(ga.at[:, :, px], ra1.at[d - 1], rs_send.at[0], rs_recv.at[0], (z, y, px, c)).start()
    for d in range(1, ny):
        py = lax.rem(y + d, ny)
        remote(gb.at[:, py], rb1.at[d - 1], rs_send.at[1], rs_recv.at[1], (z, py, x, c)).start()
    mix_sum[...] = dot(shid[:, : 2 * hid], sgu[:half, :], (1, 1)).astype(BF).astype(F32)

    def arrive(dz, carry):
        zs = lax.rem(z - dz + nz, nz)
        group = pl.ds(zs * plane, plane)

        @pl.when(dz == 0)
        def _():
            await_bytes(recv1.at[pl.ds(0, plane - 1)], r1_sem.at[0])

        @pl.when(dz != 0)
        def _():
            await_bytes(recv1.at[pl.ds(0, plane)], r1_sem.at[dz])

        remote(recv1.at[group], fwd1.at[group], f_send, f_recv.at[dz], partner).start()
        wide[pl.ds(pl.multiple_of(zs * plane * q1, plane * q1), plane * q1), :] = (
            recv1[group].astype(F32).reshape(plane * q1, LANES)
        )
        return carry

    lax.fori_loop(0, nz, arrive, 0)

    def arrive_other(dz, carry):
        zs = lax.rem(z - dz + nz, nz)
        group = pl.ds(zs * plane, plane)
        await_bytes(fwd1.at[pl.ds(0, plane)], f_recv.at[dz])
        wide2[pl.ds(pl.multiple_of(zs * plane * q1, plane * q1), plane * q1), :] = (
            fwd1[group].astype(F32).reshape(plane * q1, LANES)
        )
        return carry

    def spread(source, base):
        for t, target in enumerate((rows, cots)):
            for r in range(CAP):
                for k in range(chunks):
                    target[
                        r * chips : (r + 1) * chips, base + k * LANES : base + (k + 1) * LANES
                    ] = source[
                        pl.ds((t * CAP + r) * chunks + k, chips, stride=q1), :
                    ].astype(BF)

    spread(wide, 0)
    lax.fori_loop(0, nz, arrive_other, 0)
    spread(wide2, half)

    for copy in loads[8:]:
        copy.wait()
    pre[...] = dot(rows[...], wgu[...], (1, 0))
    back[...] = dot(cots[...], wd[...], (1, 1))

    for r in range(CAP):
        at = pl.ds(r * chips, chips)
        gate_act, gate_slope = silu_parts(pre[at, :hid])
        up_pre = pre[at, hid:]
        grad = back[at, :]
        value = gate_act * up_pre
        hidden[at, :] = value.astype(BF)
        delta[at, :hid] = (grad * up_pre * gate_slope).astype(BF)
        delta[at, hid:] = (grad * gate_act).astype(BF)
        total = jnp.sum(value * grad, axis=1, keepdims=True)
        prod[at, :] = jnp.broadcast_to(total, (chips, LANES)).astype(BF)

    part[...] = dot(delta[...], wgu[half:, :], (1, 1)).astype(BF)
    trade_part = remote(part, part_in, p_send.at[0], p_recv.at[0], partner)
    trade_prod = remote(prod, prod_in, p_send.at[1], p_recv.at[1], partner)
    trade_part.start()
    trade_prod.start()
    own = dot(delta[...], wgu[:half, :], (1, 1)).astype(BF)
    trade_part.wait()
    trade_prod.wait()
    summed = own.astype(F32) + part_in[...].astype(F32)
    for r in range(CAP):
        for k in range(chunks):
            wide[pl.ds(r * chunks + k, chips, stride=q2), :] = summed[
                r * chips : (r + 1) * chips, k * LANES : (k + 1) * LANES
            ]

    def narrow_back(i, carry):
        block = wide[pl.ds(pl.multiple_of(i * plane * q2, plane * q2), plane * q2), :]
        send2[pl.ds(i * plane, plane)] = block.reshape(plane, q2, LANES).astype(BF)
        return carry

    lax.fori_loop(0, nz, narrow_back, 0)
    products = prod[...].astype(F32) + prod_in[...].astype(F32)
    packed = jnp.where(
        lane == 0,
        products[:chips],
        jnp.where(lane == 1, products[chips : 2 * chips], products[2 * chips :]),
    )
    prod_out[:, 0, :] = packed.astype(BF).astype(F32)
    recv2[me] = send2[me]
    prod_home[me] = prod_out[me]

    def give_back(step, carry):
        index, device = peer(step)
        remote(send2.at[index], recv2.at[me], s2_sem, r2_sem, device).start()
        remote(prod_out.at[index], prod_home.at[me], q_send, q_recv, device).start()
        return carry

    lax.fori_loop(1, chips, give_back, 0)

    await_bytes(ra1, rs_recv.at[0])
    await_bytes(rb1, rs_recv.at[1])

    def first_sum(i, carry):
        total = ga[i, :, x].astype(F32)
        other = gb[i, y].astype(F32)
        for d in range(nx - 1):
            total = total + ra1[d, i].astype(F32)
        for d in range(ny - 1):
            other = other + rb1[d, i].astype(F32)
        sa2[i] = total.astype(BF)
        sb2[i] = other.astype(BF)
        return carry

    lax.fori_loop(0, nz, first_sum, 0)
    for d in range(1, ny):
        py = lax.rem(y + d, ny)
        remote(sa2.at[:, py], ra2.at[d - 1], rs_send.at[2], rs_recv.at[2], (z, py, x, c)).start()
    for d in range(1, nx):
        px = lax.rem(x + d, nx)
        remote(sb2.at[:, px], rb2.at[d - 1], rs_send.at[3], rs_recv.at[3], (z, y, px, c)).start()

    def expert_terms(i, carry):
        at = pl.ds(pl.multiple_of(i * zrows, LANES), zrows)
        both = dot(rows[:, at], delta[...], (0, 0)).astype(BF)
        grad_gu[0, at, :] = both[:, :hid]
        grad_gu[1, at, :] = both[:, hid:]
        grad_d[:, at] = dot(hidden[...], cots[:, at], (0, 0)).astype(BF)
        return carry

    lax.fori_loop(0, nz, expert_terms, 0)
    stores = [
        pltpu.make_async_copy(src, dst, out_sem.at[i])
        for i, (src, dst) in enumerate(
            (
                (grad_gu.at[0, :half], gate_grad.at[first]),
                (grad_gu.at[0, half:], gate_grad.at[second]),
                (grad_gu.at[1, :half], up_grad.at[first]),
                (grad_gu.at[1, half:], up_grad.at[second]),
                (grad_d.at[:, :half], down_grad.at[:, first]),
                (grad_d.at[:, half:], down_grad.at[:, second]),
            )
        )
    ]
    for copy in stores:
        copy.start()

    await_bytes(ra2, rs_recv.at[2])
    await_bytes(rb2, rs_recv.at[3])

    def second_sum(i, carry):
        total = sa2[i, y].astype(F32)
        other = sb2[i, x].astype(F32)
        for d in range(ny - 1):
            total = total + ra2[d, i].astype(F32)
        for d in range(nx - 1):
            other = other + rb2[d, i].astype(F32)
        sa3[i] = total.astype(BF)
        sb3[i] = other.astype(BF)
        return carry

    lax.fori_loop(0, nz, second_sum, 0)
    for d in range(1, nz):
        pz = lax.rem(z + d, nz)
        remote(sa3.at[pz], ra3.at[d - 1], rs_send.at[4], rs_recv.at[4], (pz, y, x, c)).start()
        remote(sb3.at[pz], rb3.at[d - 1], rs_send.at[5], rs_recv.at[5], (pz, y, x, c)).start()
    trade_mix.wait()
    mix_sum[...] = mix_sum[...] + mix_in[...].astype(F32)
    await_bytes(ra3, rs_recv.at[4])
    await_bytes(rb3, rs_recv.at[5])
    total = sa3[z].astype(F32)
    other = sb3[z].astype(F32)
    for d in range(nz - 1):
        total = total + ra3[d].astype(F32)
        other = other + rb3[d].astype(F32)
    sgate_grad[...] = total[:, :hid]
    sup_grad[:, : cut - hid] = total[:, hid:]
    sup_grad[:, cut - hid :] = other[:, : 2 * hid - cut]
    sdown_grad[...] = other[:, 2 * hid - cut :]

    await_bytes(prod_home.at[pl.ds(0, chips - 1)], q_recv)
    held = onehot[...]
    seen = prod_home[:, 0, :]
    ranked = [jnp.where(lane == r, seen, 0.0).astype(BF) for r in range(CAP)]
    for k in range(2):
        mine = jnp.zeros((toks, LANES), F32)
        for r in range(CAP):
            chosen = jnp.where(picks[k], held[:, r * chips : (r + 1) * chips].astype(F32), 0.0)
            mine = mine + dot(chosen.astype(BF), ranked[r], (1, 0))
        weight_grad[:, k : k + 1] = (
            jnp.sum(mine, axis=1, keepdims=True) / route_weights[:, k : k + 1]
        )
    await_bytes(recv2.at[pl.ds(0, chips - 1)], r2_sem)
    wide[pl.ds(0, chips * q2), :] = recv2[...].astype(F32).reshape(chips * q2, LANES)
    for r in range(CAP):
        for k in range(chunks):
            home[r * chips : (r + 1) * chips, k * LANES : (k + 1) * LANES] = wide[
                pl.ds(r * chunks + k, chips, stride=q2), :
            ].astype(BF)
    token_grad[...] = (mix_sum[...] + dot(held, home[...], (1, 0))).astype(BF)

    await_bytes(send1.at[pl.ds(0, chips - 1)], s1_sem)
    await_bytes(fwd1, f_send)
    await_bytes(send2.at[pl.ds(0, chips - 1)], s2_sem)
    await_bytes(prod_out.at[pl.ds(0, chips - 1)], q_send)
    for i, ref in enumerate((ra1, rb1, ra2, rb2, ra3, rb3)):
        await_bytes(ref, rs_send.at[i])
    for copy in stores:
        copy.wait()


def per_device(
    tokens, cotangent, routes, route_weights, gate_proj, up_proj, down_proj,
    shared_gate, shared_up, shared_down,
):
    nz, ny, nx = (lax.axis_size(n) for n in EP)
    chips = nz * ny * nx
    toks, half = tokens.shape
    width = 2 * half
    hid = gate_proj.shape[2]
    slots = CAP * chips
    q1, q2 = 2 * CAP * half // LANES, CAP * half // LANES
    rblk = width // chips
    cut = 3 * hid // 2
    hbm = pl.BlockSpec(memory_space=pl.ANY)
    vmem = pl.BlockSpec(memory_space=pltpu.VMEM)
    dma = pltpu.SemaphoreType.DMA

    def kernel(*refs):
        fused_kernel(nz, ny, nx, *refs)

    outs = pl.pallas_call(
        kernel,
        out_shape=[
            jax.ShapeDtypeStruct((toks, half), BF),
            jax.ShapeDtypeStruct((toks, 2), F32),
            jax.ShapeDtypeStruct((width, hid), BF),
            jax.ShapeDtypeStruct((width, hid), BF),
            jax.ShapeDtypeStruct((hid, width), BF),
            jax.ShapeDtypeStruct((rblk, hid), F32),
            jax.ShapeDtypeStruct((rblk, hid), F32),
            jax.ShapeDtypeStruct((rblk, hid), F32),
        ],
        in_specs=[hbm, hbm, vmem, vmem] + [hbm] * 6,
        out_specs=[vmem, vmem, hbm, hbm, hbm, vmem, vmem, vmem],
        scratch_shapes=[
            pltpu.VMEM((toks, width), BF),
            pltpu.VMEM((toks, width), BF),
            pltpu.VMEM((width, 2 * hid), BF),
            pltpu.VMEM((hid, width), BF),
            pltpu.VMEM((width, 2 * hid), BF),
            pltpu.VMEM((width, hid), BF),
            pltpu.VMEM((toks, slots), BF),
            pltpu.VMEM((chips * q1, LANES), F32),
            pltpu.VMEM((chips * q1, LANES), F32),
            pltpu.VMEM((chips, q1, LANES), BF),
            pltpu.VMEM((chips, q1, LANES), BF),
            pltpu.VMEM((chips, q1, LANES), BF),
            pltpu.VMEM((slots, width), BF),
            pltpu.VMEM((slots, width), BF),
            pltpu.VMEM((slots, 2 * hid), F32),
            pltpu.VMEM((slots, hid), F32),
            pltpu.VMEM((slots, hid), BF),
            pltpu.VMEM((slots, 2 * hid), BF),
            pltpu.VMEM((slots, half), BF),
            pltpu.VMEM((slots, half), BF),
            pltpu.VMEM((slots, LANES), BF),
            pltpu.VMEM((slots, LANES), BF),
            pltpu.VMEM((chips, 1, LANES), F32),
            pltpu.VMEM((chips, 1, LANES), F32),
            pltpu.VMEM((chips, q2, LANES), BF),
            pltpu.VMEM((chips, q2, LANES), BF),
            pltpu.VMEM((slots, half), BF),
            pltpu.VMEM((toks, half), BF),
            pltpu.VMEM((toks, half), BF),
            pltpu.VMEM((toks, half), F32),
            pltpu.VMEM((toks, 2 * hid), F32),
            pltpu.VMEM((toks, 3 * hid), BF),
            pltpu.VMEM((2, width, hid), BF),
            pltpu.VMEM((hid, width), BF),
            pltpu.VMEM((nz, ny, nx, rblk, cut), BF),
            pltpu.VMEM((nz, ny, nx, rblk, cut), BF),
            pltpu.VMEM((nx - 1, nz, ny, rblk, cut), BF),
            pltpu.VMEM((ny - 1, nz, nx, rblk, cut), BF),
            pltpu.VMEM((nz, ny, rblk, cut), BF),
            pltpu.VMEM((nz, nx, rblk, cut), BF),
            pltpu.VMEM((ny - 1, nz, rblk, cut), BF),
            pltpu.VMEM((nx - 1, nz, rblk, cut), BF),
            pltpu.VMEM((nz, rblk, cut), BF),
            pltpu.VMEM((nz, rblk, cut), BF),
            pltpu.VMEM((nz - 1, rblk, cut), BF),
            pltpu.VMEM((nz - 1, rblk, cut), BF),
            dma((14,)),
            dma((2,)),
            dma((2,)),
            dma,
            dma((nz,)),
            dma,
            dma((nz,)),
            dma((2,)),
            dma((2,)),
            dma,
            dma,
            dma,
            dma,
            dma,
            dma,
            dma((6,)),
            dma((6,)),
            dma((6,)),
        ],
        compiler_params=pltpu.CompilerParams(
            collective_id=0, has_side_effects=True, vmem_limit_bytes=62 << 20
        ),
        name="fused",
    )(
        tokens, cotangent, routes, route_weights,
        gate_proj[0], up_proj[0], down_proj[0], shared_gate, shared_up, shared_down,
    )
    outs = list(outs)
    for i in (2, 3, 4):
        outs[i] = outs[i][None]
    return tuple(outs)


def solution(mesh):
    split = Mesh(mesh.devices.reshape(8, 4, 4, mesh.shape["tp"]), EP + ("tp",))
    placed = (
        P(EP, "tp"),
        P(EP, "tp"),
        P(EP, None),
        P(EP, None),
        P(EP, None, "tp"),
        P(EP, None, "tp"),
        P(EP, "tp", None),
        P(None, "tp"),
        P(None, "tp"),
        P(None, "tp"),
    )
    return jax.shard_map(
        per_device,
        mesh=split,
        in_specs=placed,
        out_specs=(
            P(EP, "tp"),
            P(EP, None),
            P(EP, None, "tp"),
            P(EP, None, "tp"),
            P(EP, "tp", None),
            P(EP, "tp"),
            P(EP, "tp"),
            P(EP, "tp"),
        ),
        check_vma=False,
    )
```

time: 265 us -> 104 us (0.39)
  waiting for transfers between devices: 129 us -> 0 us
  Pallas kernels: 0 us -> 88.9 us
  local copies, waits for them, and re-layouts: 47.4 us -> 12.3 us
  starting transfers between devices: 27.8 us -> 0 us
  other arithmetic: 19.5 us -> 0 us
  matrix products: 17.6 us -> 0 us
  between operations: 14.3 us -> 0.66 us
  blocking collectives: 9.1 us -> 0 us
    pallas_call x0 -> x1, Pallas kernels: none -> 88.9 us  [per_device(): pl.pallas_call(kernel, out_shape=[jax.ShapeDtypeStruct((toks, half), BF),...]
    all_to_all x2 -> x0, waiting for transfers between devices: 73 us -> none  [the longest x1 51.2 us: side_by_side(): lax.all_to_all(both, axis, split_axis=split_dim, concat_axis=concat_dim,...]
    reduce_scatter x1 -> x0, waiting for transfers between devices: 46.8 us -> none  [own_rows(): running = lax.psum_scatter(running, axis, scatter_dimension=0, tiled=True)]
    all_to_all x2 -> x0, starting transfers between devices: 27.4 us -> none  [the longest x1 15.8 us: side_by_side(): lax.all_to_all(both, axis, split_axis=split_dim, concat_axis=concat_dim,...]
    dot_general x16 -> x0, matrix products: 17.6 us -> none  [the longest x1 2.51 us: per_device(): jnp.einsum('erd,efd->erf', slot_cot, down_proj, preferred_element_type=jn...]
    concatenate x6 -> x0, other arithmetic: 12.5 us -> none  [the longest x1 3.56 us: per_device(): jnp.concatenate([contract_rows(whole_rows, mixgrad_gate), contract_rows(w...]
    gather x6 -> x0, local copies, waits for them, and re-layouts: 10.7 us -> none  [the longest x1 2.81 us: per_device(): route_weights.reshape(assigned)[owner_safe]]
    split x4 -> x0, local copies, waits for them, and re-layouts: 10.6 us -> none  [the longest x1 4.6 us: sent_together(): jnp.split(filled, [sum(widths[:k]) for k in range(1, len(widths))], axis=...]
  transfers between devices with their start and end apart: 7 -> 0, of which waited for: 5 -> 0; matrix products, arithmetic and copies ran while one was open for 22% -> 0% of each run, Pallas kernels for 0% -> 0%
where the time goes in v2:
time: 104 us; the launch traced here: 102 us
  Pallas kernels  88.9 us (85%)
  local copies, waits for them, and re-layouts  12.3 us (12%)
    pallas_call x1, Pallas kernels, per_device(): pl.pallas_call(kernel, out_shape=[jax.ShapeDtypeStruct((toks, half), BF),...  88.9 us
    unnamed x24, local copies, waits for them, and re-layouts  12.3 us

profile of v2, /device:TPU:8, one launch (start us, length us, event | category | flops | bytes accessed | tf_op | source)
XLA Modules:
  0.0 101.8 jit_solution(10795322933681416255)
XLA Ops:
  0.6 0.0 copy-start.5
  0.6 0.7 copy-done.5
  1.3 0.0 copy-start.6
  1.3 0.7 copy.18.refs_2_
  2.1 0.0 copy-done.6
  2.1 0.7 copy.19.refs_3_
  2.8 88.9 %fused.1 = (bf16[128,1024]{1,0:T(8,128)(2,1)}, f32[128,2]{1,0:T(8,128)}, bf16[2048,256]{1,0:T(8,128)(2,1)}, bf16[2048,256]{1,0:T(8,128)(2,1)}, bf16[256,2048]{1,...) custom-call(bf16[128,1024]{1,0:T(8,128)(2,1)} %refs_0_.1, bf16[128,1024]{1,0:T(8,128)(2,1)} %refs_1_.1, ...), custom_call_target="tpu_custom_call" | custom-call | tf_op jit(solution)/shard_map/fused/pallas_call | solution.py:425
  91.7 1.5 %copy.20 = f32[128,2]{0,1:T(2,128)} copy(f32[128,2]{1,0:T(8,128)} %get-tuple-element.25) | data formatting | bytes 2048
  93.2 1.7 %copy.28 = bf16[128,1024]{1,0:T(8,128)(2,1)} copy(bf16[128,1024]{1,0:T(8,128)(2,1)} %get-tuple-element.40) | data formatting | bytes 524288
  94.8 0.0 copy-start.1
  94.8 2.4 %copy.29 = bf16[1,2048,256]{2,1,0:T(8,128)(2,1)} copy(bf16[1,2048,256]{2,1,0:T(8,128)(2,1)} %bitcast.8) | data formatting | bytes 2097152
  97.2 0.0 copy-done.1
  97.2 0.0 copy-start
  97.2 1.0 copy.30
  98.2 0.6 copy-done
  98.8 0.0 copy-start.4
  98.8 1.0 copy.31
  99.8 0.0 copy-done.4
  99.8 0.0 copy-start.3
  99.8 0.6 copy.32
  100.4 0.1 copy-done.3
  100.5 0.0 copy-start.2
  100.5 0.6 copy.33
  101.1 0.1 copy-done.2
  101.2 0.6 copy.34
Async XLA Ops:
  0.6 0.7 copy-start.5
  1.3 0.7 copy-start.6
  94.8 2.4 %copy-start.1 = (bf16[2048,256]{1,0:T(8,128)(2,1)S(1)}, bf16[2048,256]{1,0:T(8,128)(2,1)}, u32[]{:S(2)}) copy-start(bf16[2048,256]{1,0:T(8,128)(2,1)} %get-tuple-element.19) | copy-start | bytes 3145732
  97.2 1.6 %copy-start = (bf16[256,2048]{1,0:T(8,128)(2,1)S(1)}, bf16[256,2048]{1,0:T(8,128)(2,1)}, u32[]{:S(2)}) copy-start(bf16[256,2048]{1,0:T(8,128)(2,1)} %get-tuple-element.20) | copy-start | bytes 3145732
  98.8 1.0 copy-start.4
  99.8 0.7 copy-start.3
  100.5 0.7 copy-start.2

commit v3 on v2

v3 whole, which is shorter than its diff:
```python
import jax
import jax.numpy as jnp
from jax import lax
from jax.experimental import pallas as pl
from jax.experimental.pallas import tpu as pltpu
from jax.sharding import Mesh
from jax.sharding import PartitionSpec as P

EP = ("ep_0", "ep_1", "ep_2")
BF = jnp.bfloat16
F32 = jnp.float32
CAP = 3
LANES = 128


def dot(left, right, dims):
    return lax.dot_general(left, right, ((dims[:1], dims[1:]), ((), ())), preferred_element_type=F32)


def silu_parts(preact):
    sigmoid_v = jax.nn.sigmoid(preact)
    return (preact * sigmoid_v, sigmoid_v * (1.0 + preact * (1.0 - sigmoid_v)))


def fused_kernel(
    nz, ny, nx,
    tokens, cotangent, routes_in, weights_in, gate_proj, up_proj, down_proj,
    shared_gate, shared_up, shared_down,
    token_grad, weight_grad, gate_grad, up_grad, down_grad, sgate_grad, sup_grad, sdown_grad,
    wtok, wcot, wgu, wd, sgu, sd,
    routes, route_weights, onehot, wide, wide2, send1, recv1, fwd1, rows, cots,
    pre, back, hidden, delta, part, part_in, prod, prod_in, prod_out, prod_home,
    send2, recv2, home, mix, mix_in, mix_sum, smix, shid,
    ga, gb, ra1, rb1, sa2, sb2, ra2, rb2, sa3, sb3, ra3, rb3,
    load_sem, tp_send, tp_recv, s1_sem, r1_sem, f_send, f_recv, p_send, p_recv,
    m_send, m_recv, s2_sem, r2_sem, q_send, q_recv, rs_send, rs_recv,
):
    z, y, x, c = (lax.axis_index(n) for n in EP + ("tp",))
    chips = nz * ny * nx
    plane = ny * nx
    me = (z * ny + y) * nx + x
    toks, half = tokens.shape
    width = 2 * half
    hid = wd.shape[0]
    chunks = half // LANES
    q1 = 2 * CAP * chunks
    q2 = CAP * chunks
    first = pl.ds(pl.multiple_of(c * half, LANES), half)
    second = pl.ds(pl.multiple_of((1 - c) * half, LANES), half)
    partner = (z, y, x, 1 - c)

    def remote(src, dst, send_sem, recv_sem, device):
        return pltpu.make_async_remote_copy(
            src_ref=src, dst_ref=dst, send_sem=send_sem, recv_sem=recv_sem,
            device_id=device, device_id_type=pl.DeviceIdType.MESH,
        )

    def await_bytes(ref, sem):
        pltpu.make_async_copy(ref, ref, sem).wait()

    across = [
        (py, px)
        for py in [lax.rem(y + d, ny) for d in range(ny)]
        for px in [lax.rem(x + d, nx) for d in range(nx)]
    ]

    def for_plane(pz, dz, act):
        for i, (py, px) in enumerate(across):
            if i == 0:
                pl.when(dz != 0)(lambda: act((pz, y, x, c), y * nx + x))
            else:
                act((pz, py, px, c), py * nx + px)

    barrier = pltpu.get_barrier_semaphore()

    def greet(dz, carry):
        def act(device, place):
            pl.semaphore_signal(
                barrier, inc=1, device_id=device, device_id_type=pl.DeviceIdType.MESH
            )

        for_plane(lax.rem(z + dz, nz), dz, act)
        return carry

    lax.fori_loop(0, nz, greet, 0)
    pl.semaphore_signal(barrier, inc=1, device_id=partner, device_id_type=pl.DeviceIdType.MESH)

    loads = [
        pltpu.make_async_copy(src, dst, load_sem.at[i])
        for i, (src, dst) in enumerate(
            (
                (tokens, wtok.at[:, :half]),
                (cotangent, wcot.at[:, :half]),
                (shared_gate.at[first], sgu.at[:half, :hid]),
                (shared_gate.at[second], sgu.at[half:, :hid]),
                (shared_up.at[first], sgu.at[:half, hid:]),
                (shared_up.at[second], sgu.at[half:, hid:]),
                (shared_down.at[first], sd.at[:half]),
                (shared_down.at[second], sd.at[half:]),
                (gate_proj.at[first], wgu.at[:half, :hid]),
                (gate_proj.at[second], wgu.at[half:, :hid]),
                (up_proj.at[first], wgu.at[:half, hid:]),
                (up_proj.at[second], wgu.at[half:, hid:]),
                (down_proj.at[:, first], wd.at[:, :half]),
                (down_proj.at[:, second], wd.at[:, half:]),
                (routes_in, routes),
                (weights_in, route_weights),
            )
        )
    ]
    for copy in loads[14:] + loads[:14]:
        copy.start()

    loads[14].wait()
    loads[15].wait()
    lane = lax.broadcasted_iota(jnp.int32, (chips, toks), 1)
    sub = lax.broadcasted_iota(jnp.int32, (chips, toks), 0)
    picks = [routes[k : k + 1, :] == sub for k in range(2)]
    named = picks[0].astype(F32) + picks[1].astype(F32)
    earlier = dot(named.astype(BF), (sub < lane).astype(BF), (1, 0))
    weight_of = jnp.where(picks[0], route_weights[0:1, :], 0.0) + jnp.where(
        picks[1], route_weights[1:2, :], 0.0
    )
    columns = []
    for r in range(CAP):
        held = jnp.where(earlier == float(r), named, 0.0)
        onehot[r * chips : (r + 1) * chips, :] = held.astype(BF)
        columns.append(jnp.sum(held * weight_of, axis=1, keepdims=True))

    loads[0].wait()
    loads[1].wait()
    for r in range(CAP):
        pick = onehot[r * chips : (r + 1) * chips, :]
        for t, source in enumerate((wtok, wcot)):
            chosen = dot(pick, source[:, :half], (1, 0))
            if t == 1:
                chosen = columns[r] * chosen
            for k in range(chunks):
                wide[pl.ds((t * CAP + r) * chunks + k, chips, stride=q1), :] = chosen[
                    :, k * LANES : (k + 1) * LANES
                ]

    def narrow(i, carry):
        block = wide[pl.ds(pl.multiple_of(i * plane * q1, plane * q1), plane * q1), :]
        send1[pl.ds(i * plane, plane)] = block.reshape(plane, q1, LANES).astype(BF)
        return carry

    lax.fori_loop(0, nz, narrow, 0)
    recv1[me] = send1[me]

    pl.semaphore_wait(barrier, chips)

    trade = [
        remote(ref.at[:, :half], ref.at[:, half:], tp_send.at[i], tp_recv.at[i], partner)
        for i, ref in enumerate((wtok, wcot))
    ]
    for copy in trade:
        copy.start()

    jn = nz // 2

    for g in range(2):

        def launch(j, carry):
            dz = 2 * j + g
            pz = lax.rem(z + dz, nz)

            def act(device, place):
                remote(
                    send1.at[pz * plane + place], recv1.at[me], s1_sem, r1_sem.at[dz], device
                ).start()

            for_plane(pz, dz, act)
            return carry

        lax.fori_loop(0, jn, launch, 0)

    for copy in loads[2:8]:
        copy.wait()
    for copy in trade:
        copy.wait()
    smix[...] = dot(wtok[...], sgu[...], (1, 0))
    mix_back = dot(wcot[...], sd[...], (1, 0))
    mix_act, mix_slope = silu_parts(smix[:, :hid])
    mix_up = smix[:, hid:]
    shid[:, 2 * hid :] = (mix_act * mix_up).astype(BF)
    shid[:, :hid] = (mix_back * mix_up * mix_slope).astype(BF)
    shid[:, hid : 2 * hid] = (mix_back * mix_act).astype(BF)

    zrows = width // nz
    zhalf = nz // 2
    cut = ga.shape[-1]

    def shared_terms(i, carry):
        at = pl.ds(pl.multiple_of(i * zrows, LANES), zrows)
        block = lax.rem(i + c * zhalf, nz)
        one = dot(wtok[:, at], shid[:, : 2 * hid], (0, 0)).astype(BF)
        two = dot(wcot[:, at], shid[:, 2 * hid :], (0, 0)).astype(BF)
        ga[block] = one[:, :cut].reshape(ny, nx, zrows // plane, cut)
        gb[block, :, :, :, : 2 * hid - cut] = one[:, cut:].reshape(
            ny, nx, zrows // plane, 2 * hid - cut
        )
        gb[block, :, :, :, 2 * hid - cut :] = two.reshape(ny, nx, zrows // plane, hid)
        return carry

    lax.fori_loop(0, nz, shared_terms, 0)

    mix[...] = dot(shid[:, : 2 * hid], sgu[half:, :], (1, 1)).astype(BF)
    trade_mix = remote(mix, mix_in, m_send, m_recv, partner)
    trade_mix.start()
    for d in range(1, nx):
        px = lax.rem(x + d, nx)
        remote(ga.at[:, :, px], ra1.at[d - 1], rs_send.at[0], rs_recv.at[0], (z, y, px, c)).start()
    for d in range(1, ny):
        py = lax.rem(y + d, ny)
        remote(gb.at[:, py], rb1.at[d - 1], rs_send.at[1], rs_recv.at[1], (z, py, x, c)).start()
    mix_sum[...] = dot(shid[:, : 2 * hid], sgu[:half, :], (1, 1)).astype(BF).astype(F32)

    def reduce_once():
        await_bytes(ra1, rs_recv.at[0])
        await_bytes(rb1, rs_recv.at[1])

        def first_sum(i, carry):
            total = ga[i, :, x].astype(F32)
            other = gb[i, y].astype(F32)
            for d in range(nx - 1):
                total = total + ra1[d, i].astype(F32)
            for d in range(ny - 1):
                other = other + rb1[d, i].astype(F32)
            sa2[i] = total.astype(BF)
            sb2[i] = other.astype(BF)
            return carry

        lax.fori_loop(0, nz, first_sum, 0)
        for d in range(1, ny):
            py = lax.rem(y + d, ny)
            remote(sa2.at[:, py], ra2.at[d - 1], rs_send.at[2], rs_recv.at[2], (z, py, x, c)).start()
        for d in range(1, nx):
            px = lax.rem(x + d, nx)
            remote(sb2.at[:, px], rb2.at[d - 1], rs_send.at[3], rs_recv.at[3], (z, y, px, c)).start()

    count = jn * plane

    def group_step(g, meanwhile):
        def arrive(j, carry):
            dz = 2 * j + g
            zs = lax.rem(z - dz + nz, nz)
            group = pl.ds(zs * plane, plane)
            if g == 0:

                @pl.when(dz == 0)
                def _():
                    await_bytes(recv1.at[pl.ds(0, plane - 1)], r1_sem.at[0])

                @pl.when(dz != 0)
                def _():
                    await_bytes(recv1.at[pl.ds(0, plane)], r1_sem.at[dz])
            else:
                await_bytes(recv1.at[pl.ds(0, plane)], r1_sem.at[dz])

            remote(
                recv1.at[group], fwd1.at[group], f_send, f_recv.at[dz], partner
            ).start()
            wide[pl.ds(pl.multiple_of(j * plane * q1, plane * q1), plane * q1), :] = (
                recv1[group].astype(F32).reshape(plane * q1, LANES)
            )
            return carry

        lax.fori_loop(0, jn, arrive, 0)

        def spread(source, base):
            for t, target in enumerate((rows, cots)):
                for r in range(CAP):
                    for k in range(chunks):
                        target[
                            (g * CAP + r) * count : (g * CAP + r + 1) * count,
                            base + k * LANES : base + (k + 1) * LANES,
                        ] = source[
                            pl.ds((t * CAP + r) * chunks + k, count, stride=q1), :
                        ].astype(BF)

        spread(wide, 0)
        meanwhile()

        def arrive_other(j, carry):
            dz = 2 * j + g
            zs = lax.rem(z - dz + nz, nz)
            group = pl.ds(zs * plane, plane)
            await_bytes(fwd1.at[pl.ds(0, plane)], f_recv.at[dz])
            wide2[pl.ds(pl.multiple_of(j * plane * q1, plane * q1), plane * q1), :] = (
                fwd1[group].astype(F32).reshape(plane * q1, LANES)
            )
            return carry

        lax.fori_loop(0, jn, arrive_other, 0)
        spread(wide2, half)

        if g == 0:
            for copy in loads[8:14]:
                copy.wait()
        mine = pl.ds(g * CAP * count, CAP * count)
        pre[...] = dot(rows[mine, :], wgu[...], (1, 0))
        back[...] = dot(cots[mine, :], wd[...], (1, 1))
        for r in range(CAP):
            here = pl.ds(r * count, count)
            at = pl.ds((g * CAP + r) * count, count)
            gate_act, gate_slope = silu_parts(pre[here, :hid])
            up_pre = pre[here, hid:]
            grad = back[here, :]
            value = gate_act * up_pre
            hidden[at, :] = value.astype(BF)
            delta[at, :hid] = (grad * up_pre * gate_slope).astype(BF)
            delta[at, hid:] = (grad * gate_act).astype(BF)
            total = jnp.sum(value * grad, axis=1, keepdims=True)
            prod[g, here, :] = jnp.broadcast_to(total, (count, LANES)).astype(BF)

        trade_prod = remote(prod.at[g], prod_in.at[g], p_send.at[2 * g], p_recv.at[2 * g], partner)
        trade_prod.start()
        part[g] = dot(delta[mine, :], wgu[half:, :], (1, 1)).astype(BF)
        trade_part = remote(
            part.at[g], part_in.at[g], p_send.at[2 * g + 1], p_recv.at[2 * g + 1], partner
        )
        trade_part.start()
        own = dot(delta[mine, :], wgu[:half, :], (1, 1)).astype(BF)
        trade_prod.wait()
        products = prod[g].astype(F32) + prod_in[g].astype(F32)
        lanes = lax.broadcasted_iota(jnp.int32, (count, LANES), 1)
        packed = jnp.where(
            lanes == 0,
            products[:count],
            jnp.where(lanes == 1, products[count : 2 * count], products[2 * count :]),
        )
        prod_out[g * count : (g + 1) * count, 0, :] = packed.astype(BF).astype(F32)
        trade_part.wait()
        summed = own.astype(F32) + part_in[g].astype(F32)
        for r in range(CAP):
            for k in range(chunks):
                wide[pl.ds(r * chunks + k, count, stride=q2), :] = summed[
                    r * count : (r + 1) * count, k * LANES : (k + 1) * LANES
                ]

        def narrow_back(j, carry):
            block = wide[pl.ds(pl.multiple_of(j * plane * q2, plane * q2), plane * q2), :]
            send2[pl.ds(g * count + j * plane, plane)] = block.reshape(plane, q2, LANES).astype(BF)
            return carry

        lax.fori_loop(0, jn, narrow_back, 0)
        if g == 0:
            recv2[me] = send2[y * nx + x]
            prod_home[me] = prod_out[y * nx + x]

    def give_back(g):
        def leave(j, carry):
            dz = 2 * j + g
            pz = lax.rem(z - dz + nz, nz)

            def act(device, place):
                index = g * count + j * plane + place
                remote(send2.at[index], recv2.at[me], s2_sem, r2_sem, device).start()
                remote(prod_out.at[index], prod_home.at[me], q_send, q_recv, device).start()

            for_plane(pz, dz, act)
            return carry

        lax.fori_loop(0, jn, leave, 0)

    group_step(0, lambda: None)
    give_back(0)
    trade_mix.wait()
    mix_sum[...] = mix_sum[...] + mix_in[...].astype(F32)
    group_step(1, reduce_once)
    give_back(1)
    await_bytes(ra2, rs_recv.at[2])
    await_bytes(rb2, rs_recv.at[3])

    def second_sum(i, carry):
        total = sa2[i, y].astype(F32)
        other = sb2[i, x].astype(F32)
        for d in range(ny - 1):
            total = total + ra2[d, i].astype(F32)
        for d in range(nx - 1):
            other = other + rb2[d, i].astype(F32)
        sa3[i] = total.astype(BF)
        sb3[i] = other.astype(BF)
        return carry

    lax.fori_loop(0, nz, second_sum, 0)
    for d in range(1, nz):
        pz = lax.rem(z + d, nz)
        remote(sa3.at[pz], ra3.at[d - 1], rs_send.at[4], rs_recv.at[4], (pz, y, x, c)).start()
        remote(sb3.at[pz], rb3.at[d - 1], rs_send.at[5], rs_recv.at[5], (pz, y, x, c)).start()
    def expert_terms(i, carry):
        at = pl.ds(pl.multiple_of(i * zrows, LANES), zrows)
        both = dot(rows[:, at], delta[...], (0, 0)).astype(BF)
        gate_grad[at, :] = both[:, :hid]
        up_grad[at, :] = both[:, hid:]
        down_grad[:, at] = dot(hidden[...], cots[:, at], (0, 0)).astype(BF)
        return carry

    lax.fori_loop(0, nz, expert_terms, 0)
    await_bytes(prod_home.at[pl.ds(0, chips - 1)], q_recv)
    held = onehot[...]
    seen = prod_home[:, 0, :]
    for k in range(2):
        mine = jnp.zeros((chips, toks), F32)
        for r in range(CAP):
            chosen = jnp.where(picks[k], held[r * chips : (r + 1) * chips].astype(F32), 0.0)
            mine = mine + chosen * seen[:, r : r + 1]
        weight_grad[k : k + 1, :] = (
            jnp.sum(mine, axis=0, keepdims=True) / route_weights[k : k + 1, :]
        )
    await_bytes(recv2.at[pl.ds(0, chips - 1)], r2_sem)
    wide[pl.ds(0, chips * q2), :] = recv2[...].astype(F32).reshape(chips * q2, LANES)
    for r in range(CAP):
        for k in range(chunks):
            home[r * chips : (r + 1) * chips, k * LANES : (k + 1) * LANES] = wide[
                pl.ds(r * chunks + k, chips, stride=q2), :
            ].astype(BF)
    token_grad[...] = (mix_sum[...] + dot(held, home[...], (0, 0))).astype(BF)

    await_bytes(ra3, rs_recv.at[4])
    await_bytes(rb3, rs_recv.at[5])
    total = sa3[z].astype(F32)
    other = sb3[z].astype(F32)
    for d in range(nz - 1):
        total = total + ra3[d].astype(F32)
        other = other + rb3[d].astype(F32)
    sgate_grad[...] = total[:, :hid]
    sup_grad[:, : cut - hid] = total[:, hid:]
    sup_grad[:, cut - hid :] = other[:, : 2 * hid - cut]
    sdown_grad[...] = other[:, 2 * hid - cut :]

    await_bytes(send1.at[pl.ds(0, chips - 1)], s1_sem)
    await_bytes(fwd1, f_send)
    await_bytes(send2.at[pl.ds(0, chips - 1)], s2_sem)
    await_bytes(prod_out.at[pl.ds(0, chips - 1)], q_send)
    for i, ref in enumerate((ra1, rb1, ra2, rb2, ra3, rb3)):
        await_bytes(ref, rs_send.at[i])


def store_kernel(*refs):
    sources, targets, sem = refs[:8], refs[8:16], refs[16]
    half = sources[0].shape[1]
    c = lax.axis_index("tp")
    first = pl.ds(pl.multiple_of(c * half, LANES), half)
    second = pl.ds(pl.multiple_of((1 - c) * half, LANES), half)
    pairs = [
        (sources[2].at[:half], targets[2].at[first]),
        (sources[2].at[half:], targets[2].at[second]),
        (sources[3].at[:half], targets[3].at[first]),
        (sources[3].at[half:], targets[3].at[second]),
        (sources[4].at[:, :half], targets[4].at[:, first]),
        (sources[4].at[:, half:], targets[4].at[:, second]),
    ] + [(sources[i], targets[i]) for i in (0, 1, 5, 6, 7)]
    copies = [
        pltpu.make_async_copy(src, dst, sem.at[i]) for i, (src, dst) in enumerate(pairs)
    ]
    for copy in copies:
        copy.start()
    for copy in copies:
        copy.wait()


def per_device(
    tokens, cotangent, routes, route_weights, gate_proj, up_proj, down_proj,
    shared_gate, shared_up, shared_down,
):
    nz, ny, nx = (lax.axis_size(n) for n in EP)
    chips = nz * ny * nx
    toks, half = tokens.shape
    width = 2 * half
    hid = gate_proj.shape[2]
    slots = CAP * chips
    q1, q2 = 2 * CAP * half // LANES, CAP * half // LANES
    rblk = width // chips
    cut = 3 * hid // 2
    hbm = pl.BlockSpec(memory_space=pltpu.HBM)
    vmem = pl.BlockSpec(memory_space=pltpu.VMEM)
    dma = pltpu.SemaphoreType.DMA

    finals = [
        ((toks, half), BF),
        ((2, toks), F32),
        ((width, hid), BF),
        ((width, hid), BF),
        ((hid, width), BF),
        ((rblk, hid), F32),
        ((rblk, hid), F32),
        ((rblk, hid), F32),
    ]

    def kernel(*refs):
        fused_kernel(nz, ny, nx, *refs)

    pin = lambda a: pltpu.with_memory_space_constraint(a, pltpu.HBM)
    outs = pl.pallas_call(
        kernel,
        out_shape=[jax.ShapeDtypeStruct(shape, dtype) for shape, dtype in finals],
        in_specs=[hbm] * 10,
        out_specs=[vmem] * 8,
        scratch_shapes=[
            pltpu.VMEM((toks, width), BF),
            pltpu.VMEM((toks, width), BF),
            pltpu.VMEM((width, 2 * hid), BF),
            pltpu.VMEM((hid, width), BF),
            pltpu.VMEM((width, 2 * hid), BF),
            pltpu.VMEM((width, hid), BF),
            pltpu.VMEM((2, toks), jnp.int32),
            pltpu.VMEM((2, toks), F32),
            pltpu.VMEM((slots, toks), BF),
            pltpu.VMEM((chips * q1, LANES), F32),
            pltpu.VMEM((chips * q1 // 2, LANES), F32),
            pltpu.VMEM((chips, q1, LANES), BF),
            pltpu.VMEM((chips, q1, LANES), BF),
            pltpu.VMEM((chips, q1, LANES), BF),
            pltpu.VMEM((slots, width), BF),
            pltpu.VMEM((slots, width), BF),
            pltpu.VMEM((slots // 2, 2 * hid), F32),
            pltpu.VMEM((slots // 2, hid), F32),
            pltpu.VMEM((slots, hid), BF),
            pltpu.VMEM((slots, 2 * hid), BF),
            pltpu.VMEM((2, slots // 2, half), BF),
            pltpu.VMEM((2, slots // 2, half), BF),
            pltpu.VMEM((2, slots // 2, LANES), BF),
            pltpu.VMEM((2, slots // 2, LANES), BF),
            pltpu.VMEM((chips, 1, LANES), F32),
            pltpu.VMEM((chips, 1, LANES), F32),
            pltpu.VMEM((chips, q2, LANES), BF),
            pltpu.VMEM((chips, q2, LANES), BF),
            pltpu.VMEM((slots, half), BF),
            pltpu.VMEM((toks, half), BF),
            pltpu.VMEM((toks, half), BF),
            pltpu.VMEM((toks, half), F32),
            pltpu.VMEM((toks, 2 * hid), F32),
            pltpu.VMEM((toks, 3 * hid), BF),
            pltpu.VMEM((nz, ny, nx, rblk, cut), BF),
            pltpu.VMEM((nz, ny, nx, rblk, cut), BF),
            pltpu.VMEM((nx - 1, nz, ny, rblk, cut), BF),
            pltpu.VMEM((ny - 1, nz, nx, rblk, cut), BF),
            pltpu.VMEM((nz, ny, rblk, cut), BF),
            pltpu.VMEM((nz, nx, rblk, cut), BF),
            pltpu.VMEM((ny - 1, nz, rblk, cut), BF),
            pltpu.VMEM((nx - 1, nz, rblk, cut), BF),
            pltpu.VMEM((nz, rblk, cut), BF),
            pltpu.VMEM((nz, rblk, cut), BF),
            pltpu.VMEM((nz - 1, rblk, cut), BF),
            pltpu.VMEM((nz - 1, rblk, cut), BF),
            dma((16,)),
            dma((2,)),
            dma((2,)),
            dma,
            dma((nz,)),
            dma,
            dma((nz,)),
            dma((4,)),
            dma((4,)),
            dma,
            dma,
            dma,
            dma,
            dma,
            dma,
            dma((6,)),
            dma((6,)),
        ],
        compiler_params=pltpu.CompilerParams(
            collective_id=0, has_side_effects=True, vmem_limit_bytes=48 << 20
        ),
        name="fused",
    )(
        *map(pin, (tokens, cotangent, routes.T, route_weights.T,
        gate_proj[0], up_proj[0], down_proj[0], shared_gate, shared_up, shared_down))
    )
    outs = pl.pallas_call(
        store_kernel,
        out_shape=[jax.ShapeDtypeStruct(shape, dtype) for shape, dtype in finals],
        in_specs=[vmem] * 8,
        out_specs=[hbm] * 8,
        scratch_shapes=[dma((11,))],
        compiler_params=pltpu.CompilerParams(vmem_limit_bytes=1 << 20),
        name="store",
    )(*outs)
    outs = list(outs)
    outs[1] = outs[1].T
    for i in (2, 3, 4):
        outs[i] = outs[i][None]
    return tuple(outs)


def solution(mesh):
    split = Mesh(mesh.devices.reshape(8, 4, 4, mesh.shape["tp"]), EP + ("tp",))
    placed = (
        P(EP, "tp"),
        P(EP, "tp"),
        P(EP, None),
        P(EP, None),
        P(EP, None, "tp"),
        P(EP, None, "tp"),
        P(EP, "tp", None),
        P(None, "tp"),
        P(None, "tp"),
        P(None, "tp"),
    )
    return jax.shard_map(
        per_device,
        mesh=split,
        in_specs=placed,
        out_specs=(
            P(EP, "tp"),
            P(EP, None),
            P(EP, None, "tp"),
            P(EP, None, "tp"),
            P(EP, "tp", None),
            P(EP, "tp"),
            P(EP, "tp"),
            P(EP, "tp"),
        ),
        check_vma=False,
    )
```

time: 104 us -> 79 us (0.76); the launches traced: 102 us -> 78.9 us
  local copies, waits for them, and re-layouts: 12.3 us -> 0 us
  Pallas kernels: 88.9 us -> 78.3 us
    unnamed x24 -> x0, local copies, waits for them, and re-layouts: 12.3 us -> none
    pallas_call x1 -> x2, Pallas kernels: 88.9 us -> 78.3 us  [the longest x1 76.4 us: per_device(): pl.pallas_call(kernel, out_shape=[jax.ShapeDtypeStruct(shape, dtype) for...]
where the time goes in v3:
time: 79 us; the launch traced here: 78.9 us
  Pallas kernels  78.3 us (99%)
    pallas_call x1, Pallas kernels, per_device(): pl.pallas_call(kernel, out_shape=[jax.ShapeDtypeStruct(shape, dtype) for...  76.4 us
    pallas_call x1, Pallas kernels, per_device(): pl.pallas_call(store_kernel, out_shape=[jax.ShapeDtypeStruct(shape, dtype...  1.86 us

profile of v3, /device:TPU:8, one launch (start us, length us, event | category | flops | bytes accessed | tf_op | source)
XLA Modules:
  0.0 78.9 jit_solution(5130709276902778160)
XLA Ops:
  0.6 76.4 %fused.1 = (bf16[128,1024]{1,0:T(8,128)(2,1)S(1)}, f32[2,128]{1,0:T(2,128)S(1)}, bf16[2048,256]{1,0:T(8,128)(2,1)S(1)}, bf16[2048,256]{1,0:T(8,128)(2,1)S(1)}, b...) custom-call(bf16[128,1024]{1,0:T(8,128)(2,1)} %refs_0_.1, ...), custom_call_target="tpu_custom_call" | custom-call | tf_op jit(solution)/shard_map/fused/pallas_call | solution.py:496
  77.1 1.9 %store.1 = (bf16[128,1024]{1,0:T(8,128)(2,1)}, f32[2,128]{1,0:T(2,128)}, bf16[2048,256]{1,0:T(8,128)(2,1)}, bf16[2048,256]{1,0:T(8,128)(2,1)}, bf16[256,2048]{1,...) custom-call(bf16[128,1024]{1,0:T(8,128)(2,1)S(1)} %get-tuple-element.24.refs_0_, ...), custom_call_target="tpu_custom_call" | custom-call | tf_op jit(solution)/shard_map/store/pallas_call | solution.py:574

commit v4 on v3

--- a/solution.py
+++ b/solution.py
@@ -73,7 +73,9 @@
 
     barrier = pltpu.get_barrier_semaphore()
 
-    def greet(dz, carry):
+    def greet(i, carry):
+        dz = lax.rem(i + nz // 2, nz)
+
         def act(device, place):
             pl.semaphore_signal(
                 barrier, inc=1, device_id=device, device_id_type=pl.DeviceIdType.MESH
@@ -158,11 +160,16 @@
         copy.start()
 
     jn = nz // 2
-
-    for g in range(2):
-
+    turn = nz // 2 - 2
+    home_j = (nz - turn) % nz // 2
+
+    def plane_step(j, g):
+        return lax.rem(2 * j + g + turn, nz)
+
+
+    def send_rows(g):
         def launch(j, carry):
-            dz = 2 * j + g
+            dz = plane_step(j, g)
             pz = lax.rem(z + dz, nz)
 
             def act(device, place):
@@ -174,6 +181,8 @@
             return carry
 
         lax.fori_loop(0, jn, launch, 0)
+
+    send_rows(0)
 
     for copy in loads[2:8]:
         copy.wait()
@@ -214,6 +223,7 @@
     for d in range(1, ny):
         py = lax.rem(y + d, ny)
         remote(gb.at[:, py], rb1.at[d - 1], rs_send.at[1], rs_recv.at[1], (z, py, x, c)).start()
+    send_rows(1)
     mix_sum[...] = dot(shid[:, : 2 * hid], sgu[:half, :], (1, 1)).astype(BF).astype(F32)
 
     def reduce_once():
@@ -241,9 +251,9 @@
 
     count = jn * plane
 
-    def group_step(g, meanwhile):
+    def group_step(g):
         def arrive(j, carry):
-            dz = 2 * j + g
+            dz = plane_step(j, g)
             zs = lax.rem(z - dz + nz, nz)
             group = pl.ds(zs * plane, plane)
             if g == 0:
@@ -280,10 +290,9 @@
                         ].astype(BF)
 
         spread(wide, 0)
-        meanwhile()
 
         def arrive_other(j, carry):
-            dz = 2 * j + g
+            dz = plane_step(j, g)
             zs = lax.rem(z - dz + nz, nz)
             group = pl.ds(zs * plane, plane)
             await_bytes(fwd1.at[pl.ds(0, plane)], f_recv.at[dz])
@@ -346,30 +355,48 @@
 
         lax.fori_loop(0, jn, narrow_back, 0)
         if g == 0:
-            recv2[me] = send2[y * nx + x]
-            prod_home[me] = prod_out[y * nx + x]
+            recv2[me] = send2[home_j * plane + y * nx + x]
+            prod_home[me] = prod_out[home_j * plane + y * nx + x]
 
     def give_back(g):
-        def leave(j, carry):
-            dz = 2 * j + g
-            pz = lax.rem(z - dz + nz, nz)
-
-            def act(device, place):
-                index = g * count + j * plane + place
-                remote(send2.at[index], recv2.at[me], s2_sem, r2_sem, device).start()
-                remote(prod_out.at[index], prod_home.at[me], q_send, q_recv, device).start()
-
-            for_plane(pz, dz, act)
-            return carry
-
-        lax.fori_loop(0, jn, leave, 0)
-
-    group_step(0, lambda: None)
+        def over_planes(act_on):
+            def leave(j, carry):
+                dz = plane_step(j, g)
+                pz = lax.rem(z - dz + nz, nz)
+
+                def act(device, place):
+                    act_on(g * count + j * plane + place, device)
+
+                for_plane(pz, dz, act)
+                return carry
+
+            lax.fori_loop(0, jn, leave, 0)
+
+        def product(index, device):
+            remote(prod_out.at[index], prod_home.at[me], q_send, q_recv, device).start()
+
+        def row(index, device):
+            remote(send2.at[index], recv2.at[me], s2_sem, r2_sem.at[g], device).start()
+
+        over_planes(product)
+        over_planes(row)
+
+    group_step(0)
     give_back(0)
     trade_mix.wait()
     mix_sum[...] = mix_sum[...] + mix_in[...].astype(F32)
-    group_step(1, reduce_once)
+    group_step(1)
+    reduce_once()
     give_back(1)
+    def expert_terms(i, carry):
+        at = pl.ds(pl.multiple_of(i * zrows, LANES), zrows)
+        both = dot(rows[:, at], delta[...], (0, 0)).astype(BF)
+        gate_grad[at, :] = both[:, :hid]
+        up_grad[at, :] = both[:, hid:]
+        down_grad[:, at] = dot(hidden[...], cots[:, at], (0, 0)).astype(BF)
+        return carry
+
+    lax.fori_loop(0, nz, expert_terms, 0)
     await_bytes(ra2, rs_recv.at[2])
     await_bytes(rb2, rs_recv.at[3])
 
@@ -389,15 +416,26 @@
         pz = lax.rem(z + d, nz)
         remote(sa3.at[pz], ra3.at[d - 1], rs_send.at[4], rs_recv.at[4], (pz, y, x, c)).start()
         remote(sb3.at[pz], rb3.at[d - 1], rs_send.at[5], rs_recv.at[5], (pz, y, x, c)).start()
-    def expert_terms(i, carry):
-        at = pl.ds(pl.multiple_of(i * zrows, LANES), zrows)
-        both = dot(rows[:, at], delta[...], (0, 0)).astype(BF)
-        gate_grad[at, :] = both[:, :hid]
-        up_grad[at, :] = both[:, hid:]
-        down_grad[:, at] = dot(hidden[...], cots[:, at], (0, 0)).astype(BF)
-        return carry
-
-    lax.fori_loop(0, nz, expert_terms, 0)
+    def reopen(g):
+        await_bytes(recv2.at[pl.ds(0, count - 1 + g)], r2_sem.at[g])
+
+        def plane_rows(j, carry):
+            zs = lax.rem(z + 2 * j + g, nz)
+            at = pl.ds(zs * plane, plane)
+            wide[pl.ds(pl.multiple_of(zs * plane * q2, plane * q2), plane * q2), :] = (
+                recv2[at].astype(F32).reshape(plane * q2, LANES)
+            )
+            for r in range(CAP):
+                for k in range(chunks):
+                    home[
+                        pl.ds(pl.multiple_of(r * chips + zs * plane, plane), plane),
+                        k * LANES : (k + 1) * LANES,
+                    ] = wide[pl.ds(zs * plane * q2 + r * chunks + k, plane, stride=q2), :].astype(BF)
+            return carry
+
+        lax.fori_loop(0, jn, plane_rows, 0)
+
+    reopen(0)
     await_bytes(prod_home.at[pl.ds(0, chips - 1)], q_recv)
     held = onehot[...]
     seen = prod_home[:, 0, :]
@@ -409,13 +447,7 @@
         weight_grad[k : k + 1, :] = (
             jnp.sum(mine, axis=0, keepdims=True) / route_weights[k : k + 1, :]
         )
-    await_bytes(recv2.at[pl.ds(0, chips - 1)], r2_sem)
-    wide[pl.ds(0, chips * q2), :] = recv2[...].astype(F32).reshape(chips * q2, LANES)
-    for r in range(CAP):
-        for k in range(chunks):
-            home[r * chips : (r + 1) * chips, k * LANES : (k + 1) * LANES] = wide[
-                pl.ds(r * chunks + k, chips, stride=q2), :
-            ].astype(BF)
+    reopen(1)
     token_grad[...] = (mix_sum[...] + dot(held, home[...], (0, 0))).astype(BF)
 
     await_bytes(ra3, rs_recv.at[4])
@@ -557,7 +589,7 @@
             dma,
             dma,
             dma,
-            dma,
+            dma((2,)),
             dma,
             dma,
             dma((6,)),

time: 79 us -> 74.9 us (0.948); the launches traced: 78.9 us -> 73.9 us
  Pallas kernels: 78.3 us -> 73.3 us
    pallas_call x1, Pallas kernels: 76.4 us -> 71.4 us  [per_device(): pl.pallas_call(kernel, out_shape=[jax.ShapeDtypeStruct(shape, dtype) for...]
where the time goes in v4:
time: 74.9 us; the launch traced here: 73.9 us
  Pallas kernels  73.3 us (98%)
    pallas_call x1, Pallas kernels, per_device(): pl.pallas_call(kernel, out_shape=[jax.ShapeDtypeStruct(shape, dtype) for...  71.4 us
    pallas_call x1, Pallas kernels, per_device(): pl.pallas_call(store_kernel, out_shape=[jax.ShapeDtypeStruct(shape, dtype...  1.86 us

profile of v4, /device:TPU:8, one launch (start us, length us, event | category | flops | bytes accessed | tf_op | source)
XLA Modules:
  0.0 73.9 jit_solution(12470207546644981501)
XLA Ops:
  0.6 71.4 %fused.1 = (bf16[128,1024]{1,0:T(8,128)(2,1)S(1)}, f32[2,128]{1,0:T(2,128)S(1)}, bf16[2048,256]{1,0:T(8,128)(2,1)S(1)}, bf16[2048,256]{1,0:T(8,128)(2,1)S(1)}, b...) custom-call(bf16[128,1024]{1,0:T(8,128)(2,1)} %refs_0_.1, ...), custom_call_target="tpu_custom_call" | custom-call | tf_op jit(solution)/shard_map/fused/pallas_call | solution.py:528
  72.1 1.9 %store.1 = (bf16[128,1024]{1,0:T(8,128)(2,1)}, f32[2,128]{1,0:T(2,128)}, bf16[2048,256]{1,0:T(8,128)(2,1)}, bf16[2048,256]{1,0:T(8,128)(2,1)}, bf16[256,2048]{1,...) custom-call(bf16[128,1024]{1,0:T(8,128)(2,1)S(1)} %get-tuple-element.24.refs_0_, ...), custom_call_target="tpu_custom_call" | custom-call | tf_op jit(solution)/shard_map/store/pallas_call | solution.py:606
